TPU v7x, 256 devices: a whole 4x4x8 slice. The times are simulated.
256 devices in a mesh: sp: 32 (over z, y), fs: 4 (over x), tp: 2 (over core).
Axes of the slice: x: 4, y: 4, z: 8, core: 2. Of those that a mesh axis runs over, the one named last changes fastest.
Arguments:
- tokens: bfloat16 [4, 24576, 2048], P('fs', 'sp', 'tp'), may hold values from -6 to 6
- in_gain: float32 [2048], replicated, may hold values from 0.1 to 1.9
- ret_query: bfloat16 [2048, 768], P(None, 'tp'), may hold values from -0.125 to 0.125
- ret_key: bfloat16 [2048, 768], P(None, 'tp'), may hold values from -0.125 to 0.125
- ret_value: bfloat16 [2048, 768], P(None, 'tp'), may hold values from -0.125 to 0.125
- att_query: bfloat16 [2048, 768], P(None, 'tp'), may hold values from -8 to 8
- att_key: bfloat16 [2048, 256], P(None, 'tp'), may hold values from -8 to 8
- att_value: bfloat16 [2048, 256], P(None, 'tp'), may hold values from -0.125 to 0.125
- log_decay: float32 [4, 12, 24576], P('fs', 'tp', 'sp'), may hold values from -1.5 to 0
- ret_gain: float32 [768], P('tp'), may hold values from 0.1 to 1.9
- sink_logit: float32 [12], P('tp'), may hold values from 1 to 5
- retentive_exit_matrix: bfloat16 [768, 2048], P('tp'), may hold values from -0.15625 to 0.15625
- out_att: bfloat16 [768, 2048], P('tp'), may hold values from -0.875 to 0.875
Outputs:
- mixed: bfloat16 [4, 24576, 2048], P('fs', ('sp', 'tp'))
All inputs are finite; a program needn't handle non-finite values.
Results may differ from a plain program's by a relative error of at most 0.0085.
Values may be sent and summed in bfloat16 or wider, within the bound.
No kernel may reach another device: no remote copies, remote signals or barrier semaphores. Data moves between devices by JAX's collectives and lax.ppermute only.
A program may use at most 128 MiB of HBM per device.

v0:
```python
import functools

import jax
import jax.numpy as jnp
from jax import lax
from jax.experimental import pallas as pl
from jax.experimental.pallas import tpu as pltpu
from jax.sharding import Mesh
from jax.sharding import PartitionSpec as P


HEAD_DIM = 64
WINDOW = 128
EPS = 1e-06
SP = ("sp_0", "sp_1")
SP_TP = ("sp_0", "sp_1", "tp")
F32 = jnp.float32
BF16 = jnp.bfloat16
CHUNK = 256
STATE_ROWS = 192
LOG_ROWS = 16
PAY_ROWS = STATE_ROWS + LOG_ROWS
PAIRS = 3
LANES = 128
CONTRACT_ROWS = (((0,), (0,)), ((), ()))
CONTRACT_LANES = (((1,), (1,)), ((), ()))


def dot(a, b):
    return jnp.dot(a, b, preferred_element_type=F32)


def lane_ids(shape):
    return lax.broadcasted_iota(jnp.int32, shape, len(shape) - 1)


def row_ids(shape):
    return lax.broadcasted_iota(jnp.int32, shape, 0)


def half_mask(half, dtype):
    lanes = lane_ids((1, LANES))
    inside = (lanes < HEAD_DIM) if half == 0 else (lanes >= HEAD_DIM)
    return jnp.where(inside, 1.0, 0.0).astype(dtype)


def diagonal_mask():
    return (row_ids((LANES, LANES)) < HEAD_DIM) == (lane_ids((LANES, LANES)) < HEAD_DIM)


def split3(x):
    high = x.astype(BF16).astype(F32)
    rest = x - high
    middle = rest.astype(BF16).astype(F32)
    return high, middle, rest - middle


def call(body, in_specs, out_specs, out_shape, scratch, scalars, flops, mib, grid=(1,)):
    return pl.pallas_call(
        body,
        out_shape=out_shape,
        grid_spec=pltpu.PrefetchScalarGridSpec(
            num_scalar_prefetch=scalars,
            grid=grid,
            in_specs=in_specs,
            out_specs=out_specs,
            scratch_shapes=scratch,
        ),
        compiler_params=pltpu.CompilerParams(
            dimension_semantics=("arbitrary",) * len(grid), vmem_limit_bytes=mib * 2**20
        ),
        cost_estimate=pl.CostEstimate(flops=flops, transcendentals=0, bytes_accessed=1 << 20),
    )


def whole(shape):
    return pl.BlockSpec(shape, lambda *_: (0,) * len(shape))


IN_HBM = pl.BlockSpec(memory_space=pltpu.HBM)
SCALE = HEAD_DIM**-0.5


def in_hbm(x):
    return pltpu.with_memory_space_constraint(x, pltpu.HBM)


def fetch_weights(weights, buffer, sems, begin):
    copies, start = [], 0
    depth = buffer.shape[0]
    for i, w in enumerate(weights):
        stop = start + w.shape[1]
        copy = pltpu.make_async_copy(
            w.at[pl.ds(begin, depth), :], buffer.at[:, start:stop], sems.at[i]
        )
        copy.start()
        copies.append(copy)
        start = stop
    return copies


def weight_columns(weights, begin, depth, start):
    pieces, left = [], 0
    for w in weights:
        for n in range(0, w.shape[1], LANES):
            if start <= left + n < start + CHUNK:
                pieces.append(w[pl.ds(begin, depth), n : n + LANES])
        left += w.shape[1]
    return jnp.concatenate(pieces, axis=1)


def squares_of(wide):
    squares = wide * wide
    total = squares[:, 0:LANES]
    for start in range(LANES, wide.shape[1], LANES):
        total = total + squares[:, start : start + LANES]
    return total


def decays(rates_ref, row_ref, col_ref):
    heads, _, rows = rates_ref.shape
    row_ref[...] = jnp.zeros_like(row_ref)
    for h in range(heads):
        row_ref[h : h + 1, :] = rates_ref[h]
    total = row_ref[...]
    lanes = lane_ids(total.shape)
    step = 1
    while step < rows:
        total = total + jnp.where(lanes >= step, pltpu.roll(total, step, 1), 0.0)
        step *= 2
    row_ref[...] = total
    parts = jnp.concatenate(split3(total) + (jnp.zeros_like(total),), axis=0).astype(BF16)
    shape = (32, heads * HEAD_DIM)
    picks = (row_ids(shape) % 8 == lane_ids(shape) // HEAD_DIM).astype(F32).astype(BF16)
    col_ref[...] = lax.dot_general(parts, picks, CONTRACT_ROWS, preferred_element_type=F32)


def own_body(tp, x_hbm, gain_hbm, rates_hbm, *refs):
    weights = refs[:4]
    first, scaled, sq, row, col, xbuf, gain, rates, wbuf, sems = refs[4:]
    rows, depth = xbuf.shape
    small = pltpu.make_async_copy(rates_hbm, rates, sems.at[8])
    small.start()
    load = pltpu.make_async_copy(x_hbm, xbuf, sems.at[6])
    load.start()
    gains = pltpu.make_async_copy(gain_hbm, gain, sems.at[7])
    gains.start()
    begin = pl.multiple_of(tp[0] * depth, depth)
    copies = fetch_weights(weights, wbuf, sems, begin)
    small.wait()
    decays(rates, row, col)
    gains.wait()
    load.wait()
    for copy in copies:
        copy.wait()
    scale = gain[:, pl.ds(begin, depth)]
    for m in range(0, rows, CHUNK):
        here = slice(m, m + CHUNK)
        wide = xbuf[here, :].astype(F32)
        part = (wide * scale).astype(BF16)
        scaled[here, :] = part
        sq[here, :] = squares_of(wide)
        for n in range(0, first.shape[1], CHUNK):
            first[here, n : n + CHUNK] = dot(part, wbuf[:, n : n + CHUNK])


def own_half(tp, own, gain, rates, weights):
    rows, depth = own.shape
    widths = [w.shape[1] for w in weights]
    shapes = [
        ((rows, sum(widths)), F32),
        ((rows, depth), BF16),
        ((rows, LANES), F32),
        ((8, rows), F32),
        ((rows, widths[0]), F32),
    ]
    return call(
        own_body,
        [IN_HBM] * 7,
        [whole(s) for s, _ in shapes],
        [jax.ShapeDtypeStruct(s, t) for s, t in shapes],
        [
            pltpu.VMEM((rows, depth), BF16),
            pltpu.VMEM(gain.shape, F32),
            pltpu.VMEM(rates.shape, F32),
            pltpu.VMEM((depth, sum(widths)), BF16),
            pltpu.SemaphoreType.DMA((9,)),
        ],
        1,
        2 * rows * depth * sum(widths),
        24,
    )(tp, *[in_hbm(a) for a in (own, gain, rates) + weights])


def keys_body(tp, x, gain, part, sq, col, *refs):
    weights = refs[:4]
    k_out, v_out, akv_out, inv_out, scaled_out, pay_out, tail_out = refs[4:]
    rows, depth = x.shape
    width = k_out.shape[1]
    begin = pl.multiple_of((1 - tp[0]) * depth, depth)
    scale = gain[:, pl.ds(begin, depth)]
    low = lane_ids((HEAD_DIM, LANES)) < HEAD_DIM
    for m in range(0, rows, CHUNK):
        here = slice(m, m + CHUNK)
        wide = x[here, :].astype(F32)
        scaled = (wide * scale).astype(BF16)
        scaled_out[here, :] = scaled
        mean = jnp.sum(sq[here, :] + squares_of(wide), axis=1, keepdims=True) / (2 * depth)
        inverse = lax.rsqrt(mean + EPS)
        inv_out[here, :] = jnp.broadcast_to(inverse, (CHUNK, LANES))
        for n in range(0, part.shape[1], CHUNK):
            columns = weight_columns(weights, begin, depth, n)
            total = part[here, n : n + CHUNK] + dot(scaled, columns)
            value = (total * inverse).astype(BF16)
            for j in range(n, n + CHUNK, LANES):
                piece = value[:, j - n : j - n + LANES]
                if j < width:
                    k_out[here, j : j + LANES] = piece * jnp.asarray(SCALE, BF16)
                elif j < 2 * width:
                    v_out[here, j - width : j - width + LANES] = piece
                else:
                    akv_out[here, j - 2 * width : j - 2 * width + LANES] = piece
    logs = jnp.zeros((LOG_ROWS, LANES), F32)
    places = row_ids((LOG_ROWS, LANES))
    for p in range(PAIRS):
        lanes = slice(p * LANES, (p + 1) * LANES)
        last = col[rows - 1 : rows, lanes]
        faded = (k_out[:, lanes].astype(F32) * jnp.exp(last - col[:, lanes])).astype(BF16)
        state = lax.dot_general(faded, v_out[:, lanes], CONTRACT_ROWS, preferred_element_type=F32)
        packed = jnp.where(low, state[0:HEAD_DIM], state[HEAD_DIM:]).astype(BF16)
        pay_out[p * HEAD_DIM : (p + 1) * HEAD_DIM, :] = packed
        for i, part3 in enumerate(split3(last)):
            logs = logs + jnp.where(places == 3 * p + i, part3, 0.0)
    pay_out[STATE_ROWS:, :] = logs.astype(BF16)
    tail_out[...] = akv_out[rows - WINDOW : rows, :]


def keys_half(tp, peer, gain, part, sq, col, weights):
    rows, depth = peer.shape
    widths = [w.shape[1] for w in weights]
    shapes = [
        ((rows, widths[0]), BF16),
        ((rows, widths[1]), BF16),
        ((rows, widths[2] + widths[3]), BF16),
        ((rows, LANES), F32),
        ((rows, depth), BF16),
        ((PAY_ROWS, LANES), BF16),
        ((WINDOW, widths[2] + widths[3]), BF16),
    ]
    return call(
        keys_body,
        [whole(a.shape) for a in (peer, gain, part, sq, col) + weights],
        [whole(s) for s, _ in shapes],
        [jax.ShapeDtypeStruct(s, t) for s, t in shapes],
        [],
        1,
        2 * rows * depth * sum(widths),
        20,
    )(tp, peer, gain, part, sq, col, *weights)


def queries_body(tp, own, peer, inv, w0, w1, q_out, aq_out):
    rows, depth = own.shape
    width = q_out.shape[1]
    begin = pl.multiple_of(tp[0] * depth, depth)
    other = pl.multiple_of((1 - tp[0]) * depth, depth)
    weights = (w0, w1)
    for m in range(0, rows, CHUNK):
        here = slice(m, m + CHUNK)
        inverse = inv[here, 0:1]
        for n in range(0, 2 * width, CHUNK):
            total = dot(own[here, :], weight_columns(weights, begin, depth, n))
            total = total + dot(peer[here, :], weight_columns(weights, other, depth, n))
            value = (total * inverse).astype(BF16)
            for j in range(n, n + CHUNK, LANES):
                piece = value[:, j - n : j - n + LANES]
                if j < width:
                    q_out[here, j : j + LANES] = piece
                else:
                    aq_out[here, j - width : j - width + LANES] = piece * jnp.asarray(SCALE, BF16)


def queries(tp, own, peer, inv, w0, w1):
    rows, depth = own.shape
    shapes = [(rows, w0.shape[1]), (rows, w1.shape[1])]
    return call(
        queries_body,
        [whole(a.shape) for a in (own, peer, inv, w0, w1)],
        [whole(s) for s in shapes],
        [jax.ShapeDtypeStruct(s, BF16) for s in shapes],
        [],
        1,
        8 * rows * depth * w0.shape[1],
        20,
    )(tp, own, peer, inv, w0, w1)


def inner_body(q_ref, k_ref, v_ref, row_ref, col_ref, out_ref):
    rows = q_ref.shape[0]
    later = row_ids((CHUNK, CHUNK)) >= lane_ids((CHUNK, CHUNK))
    low = lane_ids((CHUNK, LANES)) < HEAD_DIM
    diagonal = diagonal_mask()
    masks = [half_mask(0, BF16), half_mask(1, BF16)]
    for pair in range(PAIRS):
        lanes = slice(pair * LANES, (pair + 1) * LANES)
        state = start = None
        for begin in range(0, rows, CHUNK):
            here = slice(begin, begin + CHUNK)
            q, k, v = q_ref[here, lanes], k_ref[here, lanes], v_ref[here, lanes]
            cum = col_ref[here, lanes]
            parts = []
            for half in range(2):
                scores = lax.dot_general(
                    q * masks[half], k, CONTRACT_LANES, preferred_element_type=F32
                )
                over = cum[:, half * HEAD_DIM : half * HEAD_DIM + 1]
                keyed = row_ref[2 * pair + half : 2 * pair + half + 1, here]
                fade = jnp.exp(jnp.where(later, over - keyed, -jnp.inf))
                parts.append(dot((scores * fade).astype(BF16), v))
            out = jnp.where(low, parts[0], parts[1])
            end = col_ref[begin + CHUNK - 1 : begin + CHUNK, lanes]
            if state is not None:
                faded = (q.astype(F32) * jnp.exp(cum - start)).astype(BF16)
                out = out + dot(faded, state.astype(BF16))
            out_ref[here, lanes] = out
            if begin + CHUNK < rows:
                keyed = (k.astype(F32) * jnp.exp(end - cum)).astype(BF16)
                added = lax.dot_general(keyed, v, CONTRACT_ROWS, preferred_element_type=F32)
                added = jnp.where(diagonal, added, 0.0)
                state = added if state is None else state * jnp.exp(end - start) + added
                start = end


def inner(q, k, v, row, col):
    args = (q, k, v, row, col)
    return call(
        inner_body,
        [whole(a.shape) for a in args],
        whole(q.shape),
        jax.ShapeDtypeStruct(q.shape, F32),
        [],
        0,
        3 * 2**30,
        12,
    )(*args)


def logs_of(tile, p):
    return tile[3 * p : 3 * p + 1] + tile[3 * p + 1 : 3 * p + 2] + tile[3 * p + 2 : 3 * p + 3]


def state_of(ref, p):
    return ref[p * HEAD_DIM : (p + 1) * HEAD_DIM, :].astype(F32)


def log_tile(ref):
    return ref[STATE_ROWS:PAY_ROWS, :].astype(F32)


def write_logs(pay_out, rows):
    places = row_ids((LOG_ROWS, LANES))
    logs = jnp.zeros((LOG_ROWS, LANES), F32)
    for p, row in enumerate(rows):
        for i, part in enumerate(split3(row)):
            logs = logs + jnp.where(places == 3 * p + i, part, 0.0)
    pay_out[STATE_ROWS:, :] = logs.astype(BF16)


def line_body(place, *refs):
    y = place[0]
    sources, (before_out, log_out, pay_out) = refs[:4], refs[4:]
    tiles = [log_tile(r) for r in sources]
    spots = [(y - k + 4) % 4 for k in range(4)]
    lead = jnp.zeros((8, LANES), F32)
    totals = []
    for p in range(PAIRS):
        here = slice(p * HEAD_DIM, (p + 1) * HEAD_DIM)
        logs = [logs_of(t, p) for t in tiles]
        states = [state_of(r, p) for r in sources]
        total = before = between = None
        for k in range(4):
            after = jnp.zeros((1, LANES), F32)
            for j in range(4):
                if j != k:
                    after = after + jnp.where(spots[j] > spots[k], logs[j], 0.0)
            part = states[k] * jnp.exp(after)
            total = part if total is None else total + part
            if k > 0:
                part = jnp.where(k <= y, states[k], 0.0)
                part = part if between is None else part * jnp.exp(between)
                before = part if before is None else before + part
                rate = jnp.where(k <= y, logs[k], 0.0)
                between = rate if between is None else between + rate
        before_out[here, :] = before
        lead = lead + jnp.where(row_ids((8, LANES)) == p, between, 0.0)
        pay_out[here, :] = total.astype(BF16)
        totals.append(logs[0] + logs[1] + logs[2] + logs[3])
    log_out[...] = lead
    write_logs(pay_out, totals)


def column_body(place, own, back, ahead, before_out, log_out, pay_out):
    z = place[0]
    last = z == 7
    tiles = [log_tile(r) for r in (own, back, ahead)]
    lead = jnp.zeros((8, LANES), F32)
    totals = []
    for p in range(PAIRS):
        here = slice(p * HEAD_DIM, (p + 1) * HEAD_DIM)
        log, log_back, log_ahead = [logs_of(t, p) for t in tiles]
        before = jnp.where(z >= 1, state_of(back, p), 0.0)
        rate = jnp.where(z >= 1, log_back, 0.0)
        before_out[here, :] = before
        lead = lead + jnp.where(row_ids((8, LANES)) == p, rate, 0.0)
        inner_part = jnp.where(last, 0.0, state_of(own, p) + jnp.exp(log) * before)
        pay_out[here, :] = (state_of(ahead, p) + jnp.exp(log_ahead) * inner_part).astype(BF16)
        totals.append(log_ahead + jnp.where(last, 0.0, log + rate))
    log_out[...] = lead
    write_logs(pay_out, totals)


def scan_step(body, place, sources):
    return call(
        body,
        [whole(a.shape) for a in sources],
        [whole((STATE_ROWS, LANES)), whole((8, LANES)), whole((PAY_ROWS, LANES))],
        [
            jax.ShapeDtypeStruct((STATE_ROWS, LANES), F32),
            jax.ShapeDtypeStruct((8, LANES), F32),
            jax.ShapeDtypeStruct((PAY_ROWS, LANES), BF16),
        ],
        [],
        1,
        2**26,
        4,
    )(place, *sources)


def finish_body(side, row, q_ref, in_ref, col_ref, gain, *refs):
    line, line_log, column, column_log, three, six, out_ref = refs
    z = row[0]
    tile3, tile6 = log_tile(three), log_tile(six)
    diagonal = diagonal_mask()
    ones = jnp.where(diagonal, 1.0, 0.0).astype(BF16)
    for p in range(PAIRS):
        here = slice(p * HEAD_DIM, (p + 1) * HEAD_DIM)
        lanes = slice(p * LANES, (p + 1) * LANES)
        far = jnp.where(z >= 2, state_of(three, p), 0.0)
        rate = jnp.where(z >= 2, logs_of(tile3, p), 0.0)
        far = far + jnp.exp(rate) * jnp.where(z >= 5, state_of(six, p), 0.0)
        before = column[here, :] + jnp.exp(column_log[p : p + 1, :]) * far
        before = line[here, :] + jnp.exp(line_log[p : p + 1, :]) * before
        state = jnp.where(diagonal, jnp.concatenate([before, before], axis=0), 0.0).astype(BF16)
        carried = dot(q_ref[:, lanes], state) * jnp.exp(col_ref[:, lanes])
        retained = in_ref[:, lanes] + carried
        squares = retained * retained
        high = squares.astype(BF16)
        rest = (squares - high.astype(F32)).astype(BF16)
        mean = (dot(high, ones) + dot(rest, ones)) / HEAD_DIM
        out_ref[:, lanes] = (
            retained * lax.rsqrt(mean + EPS) * gain[lanes].reshape(1, LANES)
        ).astype(BF16)


def finish(mine, side, row, q, inside, col, gain, small):
    rows, width = q.shape
    spec = pl.BlockSpec((rows // 2, width), lambda i, t, z: (half_of(t, mine), 0))
    return call(
        finish_body,
        [spec, spec, spec, whole(gain.shape)] + [whole(s.shape) for s in small],
        whole((rows // 2, width)),
        jax.ShapeDtypeStruct((rows // 2, width), BF16),
        [],
        2,
        2**29,
        8,
    )(side, row, q, inside, col, gain, *small)


def half_of(side, mine):
    return side[0] if mine else 1 - side[0]


def window_body(mine, side, spot, q_ref, kv_ref, halo_ref, sink_ref, out_ref, ext):
    half, first = half_of(side, mine), spot[0]
    rows = q_ref.shape[0]
    begin = pl.multiple_of(half * rows, WINDOW)

    @pl.when(half == 0)
    def _():
        ext[0:WINDOW, :] = halo_ref[...]

    @pl.when(half == 1)
    def _():
        ext[0:WINDOW, :] = kv_ref[rows - WINDOW : rows, :]

    ext[WINDOW:, :] = kv_ref[pl.ds(begin, rows), :]
    masks = [half_mask(0, BF16), half_mask(1, BF16)]
    heads = q_ref.shape[1] // HEAD_DIM
    group = heads // 2
    band = (2 * WINDOW, group * WINDOW)
    place = lane_ids(band) % WINDOW
    distance = WINDOW + place - row_ids(band)
    near = (distance >= 0) & (distance < WINDOW)
    spot = lane_ids((1, group * WINDOW)) // WINDOW
    for block in range(rows // WINDOW):
        span = slice(block * WINDOW, (block + 2) * WINDOW)
        keys, values = ext[span, 0:LANES], ext[span, LANES:]
        allowed = near
        if block == 0:
            behind_rows = jnp.where((half == 0) & (first == 0), WINDOW, 0)
            allowed = near & (row_ids(band) >= behind_rows)
        here = slice(block * WINDOW, (block + 1) * WINDOW)
        outs = []
        for g in range(2):
            stack = []
            sink = jnp.zeros((1, group * WINDOW), F32)
            for j in range(group):
                h = g * group + j
                q = q_ref[here, h // 2 * LANES : (h // 2 + 1) * LANES]
                if h % 2 != g:
                    q = pltpu.roll(q.astype(F32), HEAD_DIM, 1).astype(BF16)
                stack.append(q * masks[g])
                sink = sink + jnp.where(spot == j, sink_ref[h], 0.0)
            scores = lax.dot_general(
                keys, jnp.concatenate(stack, axis=0), CONTRACT_LANES, preferred_element_type=F32
            )
            scores = jnp.where(allowed, scores, -jnp.inf)
            highest = jnp.maximum(jnp.max(scores, axis=0, keepdims=True), sink)
            raised = jnp.exp(scores - highest)
            total = jnp.sum(raised, axis=0, keepdims=True) + jnp.exp(sink - highest)
            weights = (raised * (1.0 / total)).astype(BF16)
            out = lax.dot_general(values, weights, CONTRACT_ROWS, preferred_element_type=F32)
            out = out[g * HEAD_DIM : (g + 1) * HEAD_DIM]
            outs += [out[:, j * WINDOW : (j + 1) * WINDOW] for j in range(group)]
        for p in range(heads // 2):
            both = jnp.concatenate([outs[2 * p], outs[2 * p + 1]], axis=0)
            out_ref[here, p * LANES : (p + 1) * LANES] = both.T.astype(BF16)


def window(mine, side, spot, q, kv, halo, sinks):
    rows, width = q.shape
    return call(
        functools.partial(window_body, mine),
        [
            pl.BlockSpec((rows // 2, width), lambda i, t, f: (half_of(t, mine), 0)),
            whole(kv.shape),
            whole(halo.shape),
            pl.BlockSpec(memory_space=pltpu.SMEM),
        ],
        whole((rows // 2, width)),
        jax.ShapeDtypeStruct((rows // 2, width), BF16),
        [pltpu.VMEM((rows // 2 + WINDOW, kv.shape[1]), BF16)],
        2,
        2**30,
        8,
    )(side, spot, q, kv, halo, sinks)


def first_exit_body(a, b, wa, wb, out):
    rows = jnp.concatenate([a[...], b[...]], axis=1)
    for n in range(0, out.shape[1], CHUNK):
        here = slice(n, n + CHUNK)
        out[:, here] = dot(rows, jnp.concatenate([wa[:, here], wb[:, here]], axis=0))


def own_exit_body(a, w, more, out):
    for n in range(0, out.shape[1], CHUNK):
        here = slice(n, n + CHUNK)
        out[:, here] = more[:, here] + dot(a[...], w[:, here])


def last_exit_body(a, w, more, out, buffer, sems):
    copies = []
    for i, n in enumerate(range(0, out.shape[1], CHUNK)):
        here = slice(n, n + CHUNK)
        buffer[:, here] = (more[:, here] + dot(a[...], w[:, here])).astype(BF16)
        copy = pltpu.make_async_copy(buffer.at[:, here], out.at[:, here], sems.at[i])
        copy.start()
        copies.append(copy)
    for copy in copies:
        copy.wait()


def first_exit(a, b, wa, wb):
    args = (a, b, wa, wb)
    shape = (a.shape[0], wa.shape[1])
    return call(
        first_exit_body,
        [whole(x.shape) for x in args],
        whole(shape),
        jax.ShapeDtypeStruct(shape, F32),
        [],
        0,
        4 * a.shape[0] * a.shape[1] * wa.shape[1],
        12,
    )(*args)


def own_exit(a, w, more):
    args = (a, w, more)
    return call(
        own_exit_body,
        [whole(x.shape) for x in args],
        whole(more.shape),
        jax.ShapeDtypeStruct(more.shape, F32),
        [],
        0,
        2 * a.shape[0] * a.shape[1] * w.shape[1],
        12,
    )(*args)


def last_exit(a, w, more):
    args = (a, w, more)
    shape = (a.shape[0], w.shape[1])
    return call(
        last_exit_body,
        [whole(x.shape) for x in args],
        IN_HBM,
        jax.ShapeDtypeStruct(shape, BF16),
        [pltpu.VMEM(shape, BF16), pltpu.SemaphoreType.DMA((shape[1] // CHUNK,))],
        0,
        2 * a.shape[0] * a.shape[1] * w.shape[1],
        14,
    )(*args)


def turned(value, axis, by):
    peers = lax.axis_size(axis)
    return lax.ppermute(value, axis, [(i, (i + by) % peers) for i in range(peers)])


def shards(
    tokens,
    in_gain,
    ret_query,
    ret_key,
    ret_value,
    att_query,
    att_key,
    att_value,
    log_decay,
    ret_gain,
    sink_logit,
    retentive_exit_matrix,
    out_att,
):
    tp = lax.axis_index("tp").astype(jnp.int32)
    y = lax.axis_index("sp_1").astype(jnp.int32)
    z = lax.axis_index("sp_0").astype(jnp.int32)
    side, spot, row = tp.reshape(1), lax.axis_index(SP).astype(jnp.int32).reshape(1), z.reshape(1)
    side, spot, row, line_spot = lax.optimization_barrier((side, spot, row, y.reshape(1)))
    own = tokens[0]
    gain = in_gain[None]
    peer = turned(own, "tp", 1)
    early = (ret_key, ret_value, att_key, att_value)
    rates = log_decay.reshape(log_decay.shape[1], 1, log_decay.shape[2])
    first, scaled_own, squares, row_cum, col = own_half(side, own, gain, rates, early)
    ret_k, ret_v, att_kv, inv, scaled, payload, tail = keys_half(
        side, peer, gain, first, squares, col, early
    )
    sources = [payload] + [turned(payload, "sp_1", k) for k in (1, 2, 3)]
    peers = lax.axis_size(SP)
    halo = lax.ppermute(tail, SP, [(i, (i + 1) % peers) for i in range(peers)])
    ret_q, att_q = queries(side, scaled_own, scaled, inv, ret_query, att_query)
    sources, ret_q = lax.optimization_barrier((sources, ret_q))
    line, line_log, span = scan_step(line_body, line_spot, sources)
    sources = [span, turned(span, "sp_0", 1), turned(span, "sp_0", 7)]
    side, span = lax.optimization_barrier((side, span))
    theirs = window(False, side, spot, att_q, att_kv, halo, sink_logit)
    exit_own, out_own, sources[0] = lax.optimization_barrier(
        (retentive_exit_matrix, out_att, sources[0])
    )
    out_peer = turned(out_own, "tp", 1)
    exit_peer = turned(exit_own, "tp", 1)
    sources, theirs = lax.optimization_barrier((sources, theirs))
    att_got = turned(theirs, "tp", 1)
    column, column_log, span = scan_step(column_body, row, sources)
    sources = [turned(span, "sp_0", 3), turned(span, "sp_0", 6)]
    side, row, span = lax.optimization_barrier((side, row, span))
    att_mine = window(True, side, spot, att_q, att_kv, halo, sink_logit)
    ret_q, row = lax.optimization_barrier((ret_q, row))
    inside = inner(ret_q, ret_k, ret_v, row_cum, col)
    partial = first_exit(att_mine, att_got, out_att, out_peer)
    sources, partial, inside = lax.optimization_barrier((sources, partial, inside))
    small = [line, line_log, column, column_log] + sources
    args = (side, row, ret_q, inside, col, ret_gain, small)
    ret_got = turned(finish(False, *args), "tp", 1)
    ret_mine = finish(True, *args)
    partial = own_exit(ret_mine, retentive_exit_matrix, partial)
    mixed = last_exit(ret_got, exit_peer, partial)
    return mixed[None]


def solution(mesh):
    finer = Mesh(
        mesh.devices.reshape(8, 4, mesh.shape["fs"], mesh.shape["tp"]), ("sp_0", "sp_1", "fs", "tp")
    )
    placed = (
        P("fs", SP, "tp"),
        P(),
        P(None, "tp"),
        P(None, "tp"),
        P(None, "tp"),
        P(None, "tp"),
        P(None, "tp"),
        P(None, "tp"),
        P("fs", "tp", SP),
        P("tp"),
        P("tp"),
        P("tp", None),
        P("tp", None),
    )
    return jax.shard_map(
        shards, mesh=finer, in_specs=placed, out_specs=P("fs", SP_TP, None), check_vma=False
    )
```

profile of v0, /device:TPU:1, one launch (start us, length us, event | category | flops | bytes accessed | tf_op | source)
XLA Modules:
  0.0 46.6 jit_solution(13793250386853388233)
XLA Ops:
  0.0 3.2 %collective-permute-start = (bf16[768,1024]{1,0:T(8,128)(2,1)}, bf16[768,1024]{1,0:T(8,128)(2,1)S(1)}, u32[]{:S(2)}, u32[]{:S(2)}) collective-permute-start(bf16[768,1024]{1,0:T(8,128)(2,1)} %bitcast.10), channel_id=1, source_target_pairs={{0,1},{1,0},{2,3},{3,2},{4,5},{5,4},{6,7},{7,6},{8,9},{9,8},{10,11... | collective-permute-start | bytes 4718600 | tf_op jit(solution)/shard_map/ppermute | solution.py:631
  3.2 4.1 %shard_map.127 = (f32[768,1024]{1,0:T(8,128)S(1)}, bf16[768,1024]{1,0:T(8,128)(2,1)S(1)}, f32[768,128]{1,0:T(8,128)S(1)}, f32[8,768]{1,0:T(8,128)S(1)}, f32[768,384]{1,0:T(8,128)S(1)}) custom-call(s32[1]{0:T(128)} %bitcast.tp.side, bf16[768,1024]{1,0:T(8,128)(2,1)} %bitcast.11, f32[1,2048]{1,0:T(1,128)} %bitcast.8, f32[6,1,768]{2,1,0:T(1,128)} %bitcast.12, ...), custom_call_target="tpu_custom_call" | custom-call | flops 1610612736 | bytes 1048576 | tf_op jit(solution)/shard_map/pallas_call | solution.py:177
  7.4 2.4 %shard_map.128 = (bf16[768,384]{1,0:T(8,128)(2,1)S(1)}, bf16[768,384]{1,0:T(8,128)(2,1)S(1)}, bf16[768,256]{1,0:T(8,128)(2,1)S(1)}, f32[768,128]{1,0:T(8,128)S(1...) custom-call(s32[1]{0:T(128)} %bitcast.tp.side, ...), custom_call_target="tpu_custom_call" | custom-call | flops 1610612736 | bytes 1048576 | tf_op jit(solution)/shard_map/pallas_call | solution.py:250
  9.8 1.1 %collective-permute-start.3 = (bf16[208,128]{1,0:T(8,128)(2,1)S(1)}, bf16[208,128]{1,0:T(8,128)(2,1)S(1)}, u32[]{:S(2)}, u32[]{:S(2)}) collective-permute-start(bf16[208,128]{1,0:T(8,128)(2,1)S(1)} %get-tuple-element.60.refs_0_), channel_id=1, source_target_pairs={{0,24},{8,0},{16,8},{24,16},{1,25},{9,1},{17,9},{25,17},{2,26},{10... | collective-permute-start | bytes 159752 | tf_op jit(solution)/shard_map/ppermute | solution.py:631
  10.9 0.3 collective-permute-start.2
  11.3 0.7 %collective-permute-start.1 = (bf16[208,128]{1,0:T(8,128)(2,1)S(1)}, bf16[208,128]{1,0:T(8,128)(2,1)S(1)}, u32[]{:S(2)}, u32[]{:S(2)}) collective-permute-start(bf16[208,128]{1,0:T(8,128)(2,1)S(1)} %get-tuple-element.60.refs_0_), channel_id=1, source_target_pairs={{0,8},{8,16},{16,24},{24,0},{1,9},{9,17},{17,25},{25,1},{2,10},{10... | collective-permute-start | bytes 159752 | tf_op jit(solution)/shard_map/ppermute | solution.py:631
  12.0 2.7 %shard_map.129 = (bf16[768,384]{1,0:T(8,128)(2,1)S(1)}, bf16[768,384]{1,0:T(8,128)(2,1)S(1)}) custom-call(s32[1]{0:T(128)} %bitcast.tp.side, bf16[768,1024]{1,0:T(8,128)(2,1)S(1)} %get-tuple-element.56.own, bf16[768,1024]{1,0:T(8,128)(2,1)S(1)} %get-tuple-element.57.peer, f32[768,128]{1,0:T(8,128)S(1)} %get-tuple-element.58.inv, ...), custom_call_target="tpu_custom_call" | custom-call | flops 2415919104 | bytes 1048576 | tf_op jit(solution)/shard_map/pallas_call | solution.py:286
  14.7 0.8 %collective-permute-done.2.refs_2_ = bf16[208,128]{1,0:T(8,128)(2,1)S(1)} collective-permute-done((bf16[208,128]{1,0:T(8,128)(2,1)S(1)}, bf16[208,128]{1,0:T(8,128)(2,1)S(1)}, u32[]{:S(2)}, u32[]{:S(2)}) %collective-permute-start.2) | collective-permute-done | bytes 53280 | tf_op jit(solution)/shard_map/ppermute | solution.py:631
  15.5 1.8 %collective-permute-done.1.refs_1_ = bf16[208,128]{1,0:T(8,128)(2,1)S(1)} collective-permute-done((bf16[208,128]{1,0:T(8,128)(2,1)S(1)}, bf16[208,128]{1,0:T(8,128)(2,1)S(1)}, u32[]{:S(2)}, u32[]{:S(2)}) %collective-permute-start.1) | collective-permute-done | bytes 53280 | tf_op jit(solution)/shard_map/ppermute | solution.py:631
  17.2 0.1 shard_map.130
  17.4 0.7 %collective-permute-start.10 = (bf16[384,2048]{1,0:T(8,128)(2,1)S(1)}, bf16[384,2048]{1,0:T(8,128)(2,1)S(1)}, u32[]{:S(2)}, u32[]{:S(2)}) collective-permute-start(bf16[384,2048]{1,0:T(8,128)(2,1)S(1)} %copy-done.2), channel_id=1, source_target_pairs={{0,1},{1,0},{2,3},{3,2},{4,5},{5,4},{6,7},{7,6},{8,9},{9,8},{10,11... | collective-permute-start | bytes 4718600 | tf_op jit(solution)/shard_map/ppermute | solution.py:631
  18.1 5.6 %collective-permute-start.5 = (bf16[208,128]{1,0:T(8,128)(2,1)S(1)}, bf16[208,128]{1,0:T(8,128)(2,1)S(1)}, u32[]{:S(2)}, u32[]{:S(2)}) collective-permute-start(bf16[208,128]{1,0:T(8,128)(2,1)S(1)} %get-tuple-element.72.own), channel_id=1, source_target_pairs={{0,224},{32,0},{64,32},{96,64},{128,96},{160,128},{192,160},{224,1... | collective-permute-start | bytes 159752 | tf_op jit(solution)/shard_map/ppermute | solution.py:631
  23.7 2.1 %collective-permute-done.6.halo_ref = bf16[128,256]{1,0:T(8,128)(2,1)S(1)} collective-permute-done((bf16[128,256]{1,0:T(8,128)(2,1)S(1)}, bf16[128,256]{1,0:T(8,128)(2,1)S(1)}, u32[]{:S(2)}, u32[]{:S(2)}) %collective-permute-start.6) | collective-permute-done | bytes 65568 | tf_op jit(solution)/shard_map/ppermute | solution.py:665
  25.8 2.9 %shard_map.131 = bf16[384,384]{1,0:T(8,128)(2,1)S(1)} custom-call(s32[1]{0:T(128)} %bitcast.tp.side, s32[1]{0:T(128)} %bitcast.1.spot, bf16[768,384]{1,0:T(8,128)(2,1)S(1)} %get-tuple-element.69.q_ref, bf16[768,256]{1,0:T(8,128)(2,1)S(1)} %get-tuple-element.70.kv_ref, bf16[128,256]{1,0:T(8,128)(2,1)S(1)} %collective-permute-done.6.halo_ref, f32[6]{0:T(128)S(1)} %copy-done.10), custom_call_target="tpu_custom_call" | custom-call | flops 1073741824 | bytes 1048576 | tf_op jit(solution)/shard_map/pallas_call | solution.py:543
  28.8 3.7 %collective-permute-start.8 = (bf16[208,128]{1,0:T(8,128)(2,1)S(1)}, bf16[208,128]{1,0:T(8,128)(2,1)S(1)}, u32[]{:S(2)}, u32[]{:S(2)}) collective-permute-start(bf16[208,128]{1,0:T(8,128)(2,1)S(1)} %get-tuple-element.75), channel_id=1, source_target_pairs={{0,192},{32,224},{64,0},{96,32},{128,64},{160,96},{192,128},{224,1... | collective-permute-start | bytes 159752 | tf_op jit(solution)/shard_map/ppermute | solution.py:631
  32.5 1.9 %collective-permute-start.9 = (bf16[384,384]{1,0:T(8,128)(2,1)S(1)}, bf16[384,384]{1,0:T(8,128)(2,1)S(1)}, u32[]{:S(2)}, u32[]{:S(2)}) collective-permute-start(bf16[384,384]{1,0:T(8,128)(2,1)S(1)} %shard_map.131), channel_id=1, source_target_pairs={{0,1},{1,0},{2,3},{3,2},{4,5},{5,4},{6,7},{7,6},{8,9},{9,8},{10,11... | collective-permute-start | bytes 884744 | tf_op jit(solution)/shard_map/ppermute | solution.py:631
  34.4 2.9 %shard_map.133.a = bf16[384,384]{1,0:T(8,128)(2,1)S(1)} custom-call(s32[1]{0:T(128)} %bitcast.tp.side, s32[1]{0:T(128)} %bitcast.1.spot, bf16[768,384]{1,0:T(8,128)(2,1)S(1)} %get-tuple-element.69.q_ref, bf16[768,256]{1,0:T(8,128)(2,1)S(1)} %get-tuple-element.70.kv_ref, bf16[128,256]{1,0:T(8,128)(2,1)S(1)} %collective-permute-done.6.halo_ref, f32[6]{0:T(128)S(1)} %copy-done.10), custom_call_target="tpu_custom_call" | custom-call | flops 1073741824 | bytes 1048576 | tf_op jit(solution)/shard_map/pallas_call | solution.py:543
  37.4 2.4 %shard_map.135.in_ref = f32[768,384]{1,0:T(8,128)S(1)} custom-call(bf16[768,384]{1,0:T(8,128)(2,1)S(1)} %get-tuple-element.80.q_ref, bf16[768,384]{1,0:T(8,128)(2,1)S(1)} %get-tuple-element.83.k_ref, bf16[768,384]{1,0:T(8,128)(2,1)S(1)} %get-tuple-element.84.v_ref, f32[8,768]{1,0:T(8,128)S(1)} %get-tuple-element.85.row_ref, ...), custom_call_target="tpu_custom_call" | custom-call | flops 3221225472 | bytes 1048576 | tf_op jit(solution)/shard_map/pallas_call | solution.py:336
  39.8 1.4 %shard_map.134.more = f32[384,2048]{1,0:T(8,128)S(1)} custom-call(bf16[384,384]{1,0:T(8,128)(2,1)S(1)} %shard_map.133.a, bf16[384,384]{1,0:T(8,128)(2,1)S(1)} %collective-permute-done.9.b, bf16[384,2048]{1,0:T(8,128)(2,1)S(1)} %copy-done.2, bf16[384,2048]{1,0:T(8,128)(2,1)S(1)} %collective-permute-done.10.wb), custom_call_target="tpu_custom_call" | custom-call | flops 1207959552 | bytes 1048576 | tf_op jit(solution)/shard_map/pallas_call | solution.py:588
  41.2 0.6 %shard_map.136 = bf16[384,384]{1,0:T(8,128)(2,1)S(1)} custom-call(s32[1]{0:T(128)} %bitcast.tp.side, s32[1]{0:T(128)} %bitcast.2.place.row, bf16[768,384]{1,0:T(8,128)(2,1)S(1)} %get-tuple-element.80.q_ref, f32[768,384]{1,0:T(8,128)S(1)} %shard_map.135.in_ref, f32[768,384]{1,0:T(8,128)S(1)} %get-tuple-element.54.col.col_ref, f32[384]{0:T(512)S(1)} %copy-done.6, ...), custom_call_target="tpu_custom_call" | custom-call | flops 536870912 | bytes 1048576 | tf_op jit(solution)/shard_map/pallas_call | solution.py:468
  41.9 0.9 %collective-permute-start.11 = (bf16[384,384]{1,0:T(8,128)(2,1)S(1)}, bf16[384,384]{1,0:T(8,128)(2,1)S(1)}, u32[]{:S(2)}, u32[]{:S(2)}) collective-permute-start(bf16[384,384]{1,0:T(8,128)(2,1)S(1)} %shard_map.136), channel_id=1, source_target_pairs={{0,1},{1,0},{2,3},{3,2},{4,5},{5,4},{6,7},{7,6},{8,9},{9,8},{10,11... | collective-permute-start | bytes 884744 | tf_op jit(solution)/shard_map/ppermute | solution.py:631
  42.8 0.6 %shard_map.137.a = bf16[384,384]{1,0:T(8,128)(2,1)S(1)} custom-call(s32[1]{0:T(128)} %bitcast.tp.side, s32[1]{0:T(128)} %bitcast.2.place.row, bf16[768,384]{1,0:T(8,128)(2,1)S(1)} %get-tuple-element.80.q_ref, f32[768,384]{1,0:T(8,128)S(1)} %shard_map.135.in_ref, f32[768,384]{1,0:T(8,128)S(1)} %get-tuple-element.54.col.col_ref, f32[384]{0:T(512)S(1)} %copy-done.6, ...), custom_call_target="tpu_custom_call" | custom-call | flops 536870912 | bytes 1048576 | tf_op jit(solution)/shard_map/pallas_call | solution.py:468
  43.5 1.0 %shard_map.138.more = f32[384,2048]{1,0:T(8,128)S(1)} custom-call(bf16[384,384]{1,0:T(8,128)(2,1)S(1)} %shard_map.137.a, bf16[384,2048]{1,0:T(8,128)(2,1)S(1)} %copy-done.3, f32[384,2048]{1,0:T(8,128)S(1)} %shard_map.134.more), custom_call_target="tpu_custom_call" | custom-call | flops 603979776 | bytes 1048576 | tf_op jit(solution)/shard_map/pallas_call | solution.py:602
  44.5 1.9 %shard_map.139 = bf16[384,2048]{1,0:T(8,128)(2,1)} custom-call(bf16[384,384]{1,0:T(8,128)(2,1)S(1)} %collective-permute-done.11.a, bf16[384,2048]{1,0:T(8,128)(2,1)S(1)} %collective-permute-done.12.w, f32[384,2048]{1,0:T(8,128)S(1)} %shard_map.138.more), custom_call_target="tpu_custom_call" | custom-call | flops 603979776 | bytes 1048576 | tf_op jit(solution)/shard_map/pallas_call | solution.py:617
  (37 shorter events, 0.3 us)
Async XLA Ops:
  0.0 7.3 %collective-permute-start = (bf16[768,1024]{1,0:T(8,128)(2,1)}, bf16[768,1024]{1,0:T(8,128)(2,1)S(1)}, u32[]{:S(2)}, u32[]{:S(2)}) collective-permute-start(bf16[768,1024]{1,0:T(8,128)(2,1)} %bitcast.10), channel_id=1, source_target_pairs={{0,1},{1,0},{2,3},{3,2},{4,5},{5,4},{6,7},{7,6},{8,9},{9,8},{10,11... | collective-permute-start | bytes 4718600 | tf_op jit(solution)/shard_map/ppermute | solution.py:631
  3.2 4.1 %copy-start = (bf16[2048,384]{1,0:T(8,128)(2,1)S(1)}, bf16[2048,384]{1,0:T(8,128)(2,1)}, u32[]{:S(2)}) copy-start(bf16[2048,384]{1,0:T(8,128)(2,1)} %refs_0_.3) | copy-start | bytes 4718596
  3.2 4.1 %copy-start.1 = (bf16[2048,384]{1,0:T(8,128)(2,1)S(1)}, bf16[2048,384]{1,0:T(8,128)(2,1)}, u32[]{:S(2)}) copy-start(bf16[2048,384]{1,0:T(8,128)(2,1)} %refs_1_.3) | copy-start | bytes 4718596
  3.2 4.1 %copy-start.4 = (bf16[2048,128]{1,0:T(8,128)(2,1)S(1)}, bf16[2048,128]{1,0:T(8,128)(2,1)}, u32[]{:S(2)}) copy-start(bf16[2048,128]{1,0:T(8,128)(2,1)} %refs_2_.3) | copy-start | bytes 1572868
  3.2 4.1 %copy-start.5 = (bf16[2048,128]{1,0:T(8,128)(2,1)S(1)}, bf16[2048,128]{1,0:T(8,128)(2,1)}, u32[]{:S(2)}) copy-start(bf16[2048,128]{1,0:T(8,128)(2,1)} %refs_3_.3) | copy-start | bytes 1572868
  3.2 4.1 %copy-start.7 = (f32[2048]{0:T(1024)S(1)}, f32[2048]{0:T(1024)}, u32[]{:S(2)}) copy-start(f32[2048]{0:T(1024)} %param.14) | copy-start | bytes 24580
  7.4 4.6 %copy-start.8 = (bf16[2048,384]{1,0:T(8,128)(2,1)S(1)}, bf16[2048,384]{1,0:T(8,128)(2,1)}, u32[]{:S(2)}) copy-start(bf16[2048,384]{1,0:T(8,128)(2,1)} %w0.1) | copy-start | bytes 4718596
  7.4 4.6 %copy-start.9 = (bf16[2048,384]{1,0:T(8,128)(2,1)S(1)}, bf16[2048,384]{1,0:T(8,128)(2,1)}, u32[]{:S(2)}) copy-start(bf16[2048,384]{1,0:T(8,128)(2,1)} %w1.1) | copy-start | bytes 4718596
  9.8 4.9 %collective-permute-start.3 = (bf16[208,128]{1,0:T(8,128)(2,1)S(1)}, bf16[208,128]{1,0:T(8,128)(2,1)S(1)}, u32[]{:S(2)}, u32[]{:S(2)}) collective-permute-start(bf16[208,128]{1,0:T(8,128)(2,1)S(1)} %get-tuple-element.60.refs_0_), channel_id=1, source_target_pairs={{0,24},{8,0},{16,8},{24,16},{1,25},{9,1},{17,9},{25,17},{2,26},{10... | collective-permute-start | bytes 159752 | tf_op jit(solution)/shard_map/ppermute | solution.py:631
  10.9 4.5 %collective-permute-start.2 = (bf16[208,128]{1,0:T(8,128)(2,1)S(1)}, bf16[208,128]{1,0:T(8,128)(2,1)S(1)}, u32[]{:S(2)}, u32[]{:S(2)}) collective-permute-start(bf16[208,128]{1,0:T(8,128)(2,1)S(1)} %get-tuple-element.60.refs_0_), channel_id=1, source_target_pairs={{0,16},{8,24},{16,0},{24,8},{1,17},{9,25},{17,1},{25,9},{2,18},{10... | collective-permute-start | bytes 159752 | tf_op jit(solution)/shard_map/ppermute | solution.py:631
  11.3 5.9 %collective-permute-start.1 = (bf16[208,128]{1,0:T(8,128)(2,1)S(1)}, bf16[208,128]{1,0:T(8,128)(2,1)S(1)}, u32[]{:S(2)}, u32[]{:S(2)}) collective-permute-start(bf16[208,128]{1,0:T(8,128)(2,1)S(1)} %get-tuple-element.60.refs_0_), channel_id=1, source_target_pairs={{0,8},{8,16},{16,24},{24,0},{1,9},{9,17},{17,25},{25,1},{2,10},{10... | collective-permute-start | bytes 159752 | tf_op jit(solution)/shard_map/ppermute | solution.py:631
  12.0 5.4 %copy-start.2 = (bf16[384,2048]{1,0:T(8,128)(2,1)S(1)}, bf16[384,2048]{1,0:T(8,128)(2,1)}, u32[]{:S(2)}) copy-start(bf16[384,2048]{1,0:T(8,128)(2,1)} %wa.1) | copy-start | bytes 4718596
  12.0 6.1 %copy-start.3 = (bf16[384,2048]{1,0:T(8,128)(2,1)S(1)}, bf16[384,2048]{1,0:T(8,128)(2,1)}, u32[]{:S(2)}) copy-start(bf16[384,2048]{1,0:T(8,128)(2,1)} %w.1) | copy-start | bytes 4718596
  12.0 13.8 %copy-start.10 = (f32[6]{0:T(128)S(1)}, f32[6]{0:T(128)}, u32[]{:S(2)}) copy-start(f32[6]{0:T(128)} %sink_ref.3) | copy-start | bytes 76
  17.4 22.4 %collective-permute-start.10 = (bf16[384,2048]{1,0:T(8,128)(2,1)S(1)}, bf16[384,2048]{1,0:T(8,128)(2,1)S(1)}, u32[]{:S(2)}, u32[]{:S(2)}) collective-permute-start(bf16[384,2048]{1,0:T(8,128)(2,1)S(1)} %copy-done.2), channel_id=1, source_target_pairs={{0,1},{1,0},{2,3},{3,2},{4,5},{5,4},{6,7},{7,6},{8,9},{9,8},{10,11... | collective-permute-start | bytes 4718600 | tf_op jit(solution)/shard_map/ppermute | solution.py:631
  18.0 26.5 %collective-permute-start.12 = (bf16[384,2048]{1,0:T(8,128)(2,1)S(1)}, bf16[384,2048]{1,0:T(8,128)(2,1)S(1)}, u32[]{:S(2)}, u32[]{:S(2)}) collective-permute-start(bf16[384,2048]{1,0:T(8,128)(2,1)S(1)} %copy-done.3), channel_id=1, source_target_pairs={{0,1},{1,0},{2,3},{3,2},{4,5},{5,4},{6,7},{7,6},{8,9},{9,8},{10,11... | collective-permute-start | bytes 4718600 | tf_op jit(solution)/shard_map/ppermute | solution.py:631
  18.1 7.6 %collective-permute-start.6 = (bf16[128,256]{1,0:T(8,128)(2,1)S(1)}, bf16[128,256]{1,0:T(8,128)(2,1)S(1)}, u32[]{:S(2)}, u32[]{:S(2)}) collective-permute-start(bf16[128,256]{1,0:T(8,128)(2,1)S(1)} %get-tuple-element.71), channel_id=1, source_target_pairs={{0,8},{8,16},{16,24},{24,32},{32,40},{40,48},{48,56},{56,64},{64,7... | collective-permute-start | bytes 196616 | tf_op jit(solution)/shard_map/ppermute | solution.py:665
  18.1 10.6 %collective-permute-start.5 = (bf16[208,128]{1,0:T(8,128)(2,1)S(1)}, bf16[208,128]{1,0:T(8,128)(2,1)S(1)}, u32[]{:S(2)}, u32[]{:S(2)}) collective-permute-start(bf16[208,128]{1,0:T(8,128)(2,1)S(1)} %get-tuple-element.72.own), channel_id=1, source_target_pairs={{0,224},{32,0},{64,32},{96,64},{128,96},{160,128},{192,160},{224,1... | collective-permute-start | bytes 159752 | tf_op jit(solution)/shard_map/ppermute | solution.py:631
  23.7 5.0 %collective-permute-start.4 = (bf16[208,128]{1,0:T(8,128)(2,1)S(1)}, bf16[208,128]{1,0:T(8,128)(2,1)S(1)}, u32[]{:S(2)}, u32[]{:S(2)}) collective-permute-start(bf16[208,128]{1,0:T(8,128)(2,1)S(1)} %get-tuple-element.72.own), channel_id=1, source_target_pairs={{0,32},{32,64},{64,96},{96,128},{128,160},{160,192},{192,224},{224... | collective-permute-start | bytes 159752 | tf_op jit(solution)/shard_map/ppermute | solution.py:631
  28.8 12.4 %collective-permute-start.8 = (bf16[208,128]{1,0:T(8,128)(2,1)S(1)}, bf16[208,128]{1,0:T(8,128)(2,1)S(1)}, u32[]{:S(2)}, u32[]{:S(2)}) collective-permute-start(bf16[208,128]{1,0:T(8,128)(2,1)S(1)} %get-tuple-element.75), channel_id=1, source_target_pairs={{0,192},{32,224},{64,0},{96,32},{128,64},{160,96},{192,128},{224,1... | collective-permute-start | bytes 159752 | tf_op jit(solution)/shard_map/ppermute | solution.py:631
  32.5 8.7 %collective-permute-start.7 = (bf16[208,128]{1,0:T(8,128)(2,1)S(1)}, bf16[208,128]{1,0:T(8,128)(2,1)S(1)}, u32[]{:S(2)}, u32[]{:S(2)}) collective-permute-start(bf16[208,128]{1,0:T(8,128)(2,1)S(1)} %get-tuple-element.75), channel_id=1, source_target_pairs={{0,96},{32,128},{64,160},{96,192},{128,224},{160,0},{192,32},{224,... | collective-permute-start | bytes 159752 | tf_op jit(solution)/shard_map/ppermute | solution.py:631
  32.5 7.3 %collective-permute-start.9 = (bf16[384,384]{1,0:T(8,128)(2,1)S(1)}, bf16[384,384]{1,0:T(8,128)(2,1)S(1)}, u32[]{:S(2)}, u32[]{:S(2)}) collective-permute-start(bf16[384,384]{1,0:T(8,128)(2,1)S(1)} %shard_map.131), channel_id=1, source_target_pairs={{0,1},{1,0},{2,3},{3,2},{4,5},{5,4},{6,7},{7,6},{8,9},{9,8},{10,11... | collective-permute-start | bytes 884744 | tf_op jit(solution)/shard_map/ppermute | solution.py:631
  39.8 1.5 %copy-start.6 = (f32[384]{0:T(512)S(1)}, f32[384]{0:T(512)}, u32[]{:S(2)}) copy-start(f32[384]{0:T(512)} %gain.3) | copy-start | bytes 4612
  41.9 2.6 %collective-permute-start.11 = (bf16[384,384]{1,0:T(8,128)(2,1)S(1)}, bf16[384,384]{1,0:T(8,128)(2,1)S(1)}, u32[]{:S(2)}, u32[]{:S(2)}) collective-permute-start(bf16[384,384]{1,0:T(8,128)(2,1)S(1)} %shard_map.136), channel_id=1, source_target_pairs={{0,1},{1,0},{2,3},{3,2},{4,5},{5,4},{6,7},{7,6},{8,9},{9,8},{10,11... | collective-permute-start | bytes 884744 | tf_op jit(solution)/shard_map/ppermute | solution.py:631
where the time goes:
time: 46.7 us; the launch traced here: 46.6 us
  Pallas kernels  23.2 us (50%)
  starting transfers between devices  18.3 us (39%)
  waiting for transfers between devices  4.62 us (10%)
    ppermute x12, starting transfers between devices, turned(): lax.ppermute(value, axis, [(i, (i + by) % peers) for i in range(peers)])  18.3 us
    pallas_call x2, Pallas kernels, window(): call(functools.partial(window_body, mine), [pl.BlockSpec((rows // 2, widt...  5.86 us
    pallas_call x1, Pallas kernels, own_half(): call(own_body, [IN_HBM] * 7, [whole(s) for s, _ in shapes], [jax.ShapeDty...  4.08 us
    pallas_call x1, Pallas kernels, queries(): call(queries_body, [whole(a.shape) for a in (own, peer, inv, w0, w1)], [w...  2.67 us
    ppermute x12, waiting for transfers between devices, turned(): lax.ppermute(value, axis, [(i, (i + by) % peers) for i in range(peers)])  2.56 us
    pallas_call x1, Pallas kernels, keys_half(): call(keys_body, [whole(a.shape) for a in (peer, gain, part, sq, col) + we...  2.43 us
    pallas_call x1, Pallas kernels, inner(): call(inner_body, [whole(a.shape) for a in args], whole(q.shape), jax.Shap...  2.42 us
    ppermute x1, waiting for transfers between devices, shards(): halo = lax.ppermute(tail, SP, [(i, (i + 1) % peers) for i in range(peers)])  2.06 us
  transfers between devices with their start and end apart: 13, of which 3 were waited for; matrix products, arithmetic and copies ran while one was open for 0% of the time, Pallas kernels for 40%

commit v1 on v0

--- a/solution.py
+++ b/solution.py
@@ -117,7 +117,7 @@
     return total
 
 
-def decays(rates_ref, row_ref, col_ref):
+def decays(rates_ref, row_ref, col_ref, wide_ref):
     heads, _, rows = rates_ref.shape
     row_ref[...] = jnp.zeros_like(row_ref)
     for h in range(heads):
@@ -130,14 +130,15 @@
         step *= 2
     row_ref[...] = total
     parts = jnp.concatenate(split3(total) + (jnp.zeros_like(total),), axis=0).astype(BF16)
-    shape = (32, heads * HEAD_DIM)
-    picks = (row_ids(shape) % 8 == lane_ids(shape) // HEAD_DIM).astype(F32).astype(BF16)
-    col_ref[...] = lax.dot_general(parts, picks, CONTRACT_ROWS, preferred_element_type=F32)
+    for ref, lanes in ((col_ref, HEAD_DIM), (wide_ref, LANES)):
+        shape = (32, heads * lanes)
+        picks = (row_ids(shape) % 8 == lane_ids(shape) // lanes).astype(F32).astype(BF16)
+        ref[...] = lax.dot_general(parts, picks, CONTRACT_ROWS, preferred_element_type=F32)
 
 
 def own_body(tp, x_hbm, gain_hbm, rates_hbm, *refs):
     weights = refs[:4]
-    first, scaled, sq, row, col, xbuf, gain, rates, wbuf, sems = refs[4:]
+    first, scaled, sq, row, col, wide_col, later, xbuf, gain, rates, wbuf, sems = refs[4:]
     rows, depth = xbuf.shape
     small = pltpu.make_async_copy(rates_hbm, rates, sems.at[8])
     small.start()
@@ -147,8 +148,10 @@
     gains.start()
     begin = pl.multiple_of(tp[0] * depth, depth)
     copies = fetch_weights(weights, wbuf, sems, begin)
+    other = pl.multiple_of((1 - tp[0]) * depth, depth)
+    more = fetch_weights(weights, later, sems.at[pl.ds(9, 4)], other)
     small.wait()
-    decays(rates, row, col)
+    decays(rates, row, col, wide_col)
     gains.wait()
     load.wait()
     for copy in copies:
@@ -162,6 +165,8 @@
         sq[here, :] = squares_of(wide)
         for n in range(0, first.shape[1], CHUNK):
             first[here, n : n + CHUNK] = dot(part, wbuf[:, n : n + CHUNK])
+    for copy in more:
+        copy.wait()
 
 
 def own_half(tp, own, gain, rates, weights):
@@ -173,6 +178,8 @@
         ((rows, LANES), F32),
         ((8, rows), F32),
         ((rows, widths[0]), F32),
+        ((rows, 2 * widths[0]), F32),
+        ((depth, sum(widths)), BF16),
     ]
     return call(
         own_body,
@@ -184,7 +191,7 @@
             pltpu.VMEM(gain.shape, F32),
             pltpu.VMEM(rates.shape, F32),
             pltpu.VMEM((depth, sum(widths)), BF16),
-            pltpu.SemaphoreType.DMA((9,)),
+            pltpu.SemaphoreType.DMA((13,)),
         ],
         1,
         2 * rows * depth * sum(widths),
@@ -192,9 +199,8 @@
     )(tp, *[in_hbm(a) for a in (own, gain, rates) + weights])
 
 
-def keys_body(tp, x, gain, part, sq, col, *refs):
-    weights = refs[:4]
-    k_out, v_out, akv_out, inv_out, scaled_out, pay_out, tail_out = refs[4:]
+def keys_body(tp, x, gain, part, sq, col, wbuf, *refs):
+    k_out, v_out, akv_out, inv_out, scaled_out, pay_out, tail_out = refs
     rows, depth = x.shape
     width = k_out.shape[1]
     begin = pl.multiple_of((1 - tp[0]) * depth, depth)
@@ -209,8 +215,7 @@
         inverse = lax.rsqrt(mean + EPS)
         inv_out[here, :] = jnp.broadcast_to(inverse, (CHUNK, LANES))
         for n in range(0, part.shape[1], CHUNK):
-            columns = weight_columns(weights, begin, depth, n)
-            total = part[here, n : n + CHUNK] + dot(scaled, columns)
+            total = part[here, n : n + CHUNK] + dot(scaled, wbuf[:, n : n + CHUNK])
             value = (total * inverse).astype(BF16)
             for j in range(n, n + CHUNK, LANES):
                 piece = value[:, j - n : j - n + LANES]
@@ -235,28 +240,27 @@
     tail_out[...] = akv_out[rows - WINDOW : rows, :]
 
 
-def keys_half(tp, peer, gain, part, sq, col, weights):
+def keys_half(tp, peer, gain, part, sq, col, wbuf, width):
     rows, depth = peer.shape
-    widths = [w.shape[1] for w in weights]
     shapes = [
-        ((rows, widths[0]), BF16),
-        ((rows, widths[1]), BF16),
-        ((rows, widths[2] + widths[3]), BF16),
+        ((rows, width), BF16),
+        ((rows, width), BF16),
+        ((rows, wbuf.shape[1] - 2 * width), BF16),
         ((rows, LANES), F32),
         ((rows, depth), BF16),
         ((PAY_ROWS, LANES), BF16),
-        ((WINDOW, widths[2] + widths[3]), BF16),
+        ((WINDOW, wbuf.shape[1] - 2 * width), BF16),
     ]
     return call(
         keys_body,
-        [whole(a.shape) for a in (peer, gain, part, sq, col) + weights],
+        [whole(a.shape) for a in (peer, gain, part, sq, col, wbuf)],
         [whole(s) for s, _ in shapes],
         [jax.ShapeDtypeStruct(s, t) for s, t in shapes],
         [],
         1,
-        2 * rows * depth * sum(widths),
+        2 * rows * depth * wbuf.shape[1],
         20,
-    )(tp, peer, gain, part, sq, col, *weights)
+    )(tp, peer, gain, part, sq, col, wbuf)
 
 
 def queries_body(tp, own, peer, inv, w0, w1, q_out, aq_out):
@@ -295,44 +299,47 @@
     )(tp, own, peer, inv, w0, w1)
 
 
-def inner_body(q_ref, k_ref, v_ref, row_ref, col_ref, out_ref):
+def inner_body(q_ref, k_ref, v_ref, row_ref, col_ref, wide_ref, out_ref):
     rows = q_ref.shape[0]
-    later = row_ids((CHUNK, CHUNK)) >= lane_ids((CHUNK, CHUNK))
-    low = lane_ids((CHUNK, LANES)) < HEAD_DIM
+    size = 256
+    later = row_ids((size, size)) >= lane_ids((size, size))
     diagonal = diagonal_mask()
     masks = [half_mask(0, BF16), half_mask(1, BF16)]
-    for pair in range(PAIRS):
-        lanes = slice(pair * LANES, (pair + 1) * LANES)
-        state = start = None
-        for begin in range(0, rows, CHUNK):
-            here = slice(begin, begin + CHUNK)
+    states = [None] * PAIRS
+    for begin in range(0, rows, size):
+        here = slice(begin, begin + size)
+        last = slice(begin + size - 1, begin + size)
+        for pair in range(PAIRS):
+            lanes = slice(pair * LANES, (pair + 1) * LANES)
             q, k, v = q_ref[here, lanes], k_ref[here, lanes], v_ref[here, lanes]
             cum = col_ref[here, lanes]
-            parts = []
+            end = col_ref[last, lanes]
+            start = col_ref[begin - 1 : begin, lanes] if begin else None
+            both = jnp.concatenate([q * masks[0], q * masks[1]], axis=0)
+            scores = lax.dot_general(both, k, CONTRACT_LANES, preferred_element_type=F32)
+            weights = []
             for half in range(2):
-                scores = lax.dot_general(
-                    q * masks[half], k, CONTRACT_LANES, preferred_element_type=F32
-                )
-                over = cum[:, half * HEAD_DIM : half * HEAD_DIM + 1]
-                keyed = row_ref[2 * pair + half : 2 * pair + half + 1, here]
-                fade = jnp.exp(jnp.where(later, over - keyed, -jnp.inf))
-                parts.append(dot((scores * fade).astype(BF16), v))
-            out = jnp.where(low, parts[0], parts[1])
-            end = col_ref[begin + CHUNK - 1 : begin + CHUNK, lanes]
-            if state is not None:
+                head = 2 * pair + half
+                over = wide_ref[here, head * LANES : (head + 1) * LANES]
+                over = jnp.concatenate([over] * (size // LANES), axis=1)
+                fade = jnp.exp(jnp.where(later, over - row_ref[head : head + 1, here], -jnp.inf))
+                part = scores[half * size : (half + 1) * size]
+                weights.append((part * fade).astype(BF16))
+            values = jnp.concatenate([v * masks[0], v * masks[1]], axis=0)
+            out = dot(jnp.concatenate(weights, axis=1), values)
+            if begin:
                 faded = (q.astype(F32) * jnp.exp(cum - start)).astype(BF16)
-                out = out + dot(faded, state.astype(BF16))
+                out = out + dot(faded, states[pair].astype(BF16))
             out_ref[here, lanes] = out
-            if begin + CHUNK < rows:
+            if begin + size < rows:
                 keyed = (k.astype(F32) * jnp.exp(end - cum)).astype(BF16)
                 added = lax.dot_general(keyed, v, CONTRACT_ROWS, preferred_element_type=F32)
                 added = jnp.where(diagonal, added, 0.0)
-                state = added if state is None else state * jnp.exp(end - start) + added
-                start = end
-
-
-def inner(q, k, v, row, col):
-    args = (q, k, v, row, col)
+                states[pair] = states[pair] * jnp.exp(end - start) + added if begin else added
+
+
+def inner(q, k, v, row, col, wide):
+    args = (q, k, v, row, col, wide)
     return call(
         inner_body,
         [whole(a.shape) for a in args],
@@ -498,18 +505,13 @@
     masks = [half_mask(0, BF16), half_mask(1, BF16)]
     heads = q_ref.shape[1] // HEAD_DIM
     group = heads // 2
-    band = (2 * WINDOW, group * WINDOW)
-    place = lane_ids(band) % WINDOW
-    distance = WINDOW + place - row_ids(band)
-    near = (distance >= 0) & (distance < WINDOW)
+    band = (WINDOW, group * WINDOW)
+    upper = row_ids(band) > lane_ids(band) % WINDOW
+    empty = jnp.where((half == 0) & (first == 0), -jnp.inf, 0.0)
     spot = lane_ids((1, group * WINDOW)) // WINDOW
     for block in range(rows // WINDOW):
         span = slice(block * WINDOW, (block + 2) * WINDOW)
         keys, values = ext[span, 0:LANES], ext[span, LANES:]
-        allowed = near
-        if block == 0:
-            behind_rows = jnp.where((half == 0) & (first == 0), WINDOW, 0)
-            allowed = near & (row_ids(band) >= behind_rows)
         here = slice(block * WINDOW, (block + 1) * WINDOW)
         outs = []
         for g in range(2):
@@ -525,13 +527,16 @@
             scores = lax.dot_general(
                 keys, jnp.concatenate(stack, axis=0), CONTRACT_LANES, preferred_element_type=F32
             )
-            scores = jnp.where(allowed, scores, -jnp.inf)
+            back = scores[0:WINDOW] + empty if block == 0 else scores[0:WINDOW]
+            scores = jnp.where(upper, back, scores[WINDOW:])
             highest = jnp.maximum(jnp.max(scores, axis=0, keepdims=True), sink)
             raised = jnp.exp(scores - highest)
             total = jnp.sum(raised, axis=0, keepdims=True) + jnp.exp(sink - highest)
-            weights = (raised * (1.0 / total)).astype(BF16)
+            weights = jnp.concatenate(
+                [jnp.where(upper, raised, 0.0), jnp.where(upper, 0.0, raised)], axis=0
+            ).astype(BF16)
             out = lax.dot_general(values, weights, CONTRACT_ROWS, preferred_element_type=F32)
-            out = out[g * HEAD_DIM : (g + 1) * HEAD_DIM]
+            out = out[g * HEAD_DIM : (g + 1) * HEAD_DIM] * (1.0 / total)
             outs += [out[:, j * WINDOW : (j + 1) * WINDOW] for j in range(group)]
         for p in range(heads // 2):
             both = jnp.concatenate([outs[2 * p], outs[2 * p + 1]], axis=0)
@@ -656,9 +661,11 @@
     peer = turned(own, "tp", 1)
     early = (ret_key, ret_value, att_key, att_value)
     rates = log_decay.reshape(log_decay.shape[1], 1, log_decay.shape[2])
-    first, scaled_own, squares, row_cum, col = own_half(side, own, gain, rates, early)
+    first, scaled_own, squares, row_cum, col, wide_col, late = own_half(
+        side, own, gain, rates, early
+    )
     ret_k, ret_v, att_kv, inv, scaled, payload, tail = keys_half(
-        side, peer, gain, first, squares, col, early
+        side, peer, gain, first, squares, col, late, ret_key.shape[1]
     )
     sources = [payload] + [turned(payload, "sp_1", k) for k in (1, 2, 3)]
     peers = lax.axis_size(SP)
@@ -681,7 +688,7 @@
     side, row, span = lax.optimization_barrier((side, row, span))
     att_mine = window(True, side, spot, att_q, att_kv, halo, sink_logit)
     ret_q, row = lax.optimization_barrier((ret_q, row))
-    inside = inner(ret_q, ret_k, ret_v, row_cum, col)
+    inside = inner(ret_q, ret_k, ret_v, row_cum, col, wide_col)
     partial = first_exit(att_mine, att_got, out_att, out_peer)
     sources, partial, inside = lax.optimization_barrier((sources, partial, inside))
     small = [line, line_log, column, column_log] + sources

time: 46.7 us -> 46.3 us (level)
  Pallas kernels: 23.2 us -> 22.2 us
  starting transfers between devices: 18.3 us -> 19 us
    ppermute x12, starting transfers between devices: 18.3 us -> 19 us  [turned(): lax.ppermute(value, axis, [(i, (i + by) % peers) for i in range(peers)])]
    pallas_call x2, Pallas kernels: 5.86 us -> 5.16 us  [window(): call(functools.partial(window_body, mine), [pl.BlockSpec((rows // 2, widt...]
  transfers between devices with their start and end apart: 13 -> 13, of which waited for: 3 -> 3; matrix products, arithmetic and copies ran while one was open for 0% -> 0% of each run, Pallas kernels for 40% -> 38%
where the time goes in v1:
time: 46.3 us; the launch traced here: 46.2 us
  Pallas kernels  22.2 us (48%)
  starting transfers between devices  19 us (41%)
  waiting for transfers between devices  4.61 us (10%)
    ppermute x12, starting transfers between devices, turned(): lax.ppermute(value, axis, [(i, (i + by) % peers) for i in range(peers)])  19 us
    pallas_call x2, Pallas kernels, window(): call(functools.partial(window_body, mine), [pl.BlockSpec((rows // 2, widt...  5.16 us
    pallas_call x1, Pallas kernels, own_half(): call(own_body, [IN_HBM] * 7, [whole(s) for s, _ in shapes], [jax.ShapeDty...  3.96 us
    pallas_call x1, Pallas kernels, queries(): call(queries_body, [whole(a.shape) for a in (own, peer, inv, w0, w1)], [w...  2.66 us
    ppermute x12, waiting for transfers between devices, turned(): lax.ppermute(value, axis, [(i, (i + by) % peers) for i in range(peers)])  2.56 us
    pallas_call x1, Pallas kernels, keys_half(): call(keys_body, [whole(a.shape) for a in (peer, gain, part, sq, col, wbuf...  2.52 us
    pallas_call x1, Pallas kernels, inner(): call(inner_body, [whole(a.shape) for a in args], whole(q.shape), jax.Shap...  2.06 us
    ppermute x1, waiting for transfers between devices, shards(): halo = lax.ppermute(tail, SP, [(i, (i + 1) % peers) for i in range(peers)])  2.06 us
  transfers between devices with their start and end apart: 13, of which 3 were waited for; matrix products, arithmetic and copies ran while one was open for 0% of the time, Pallas kernels for 38%

profile of v1, /device:TPU:1, one launch (start us, length us, event | category | flops | bytes accessed | tf_op | source)
XLA Modules:
  0.0 46.2 jit_solution(6449902893857494809)
XLA Ops:
  0.0 3.2 %collective-permute-start = (bf16[768,1024]{1,0:T(8,128)(2,1)}, bf16[768,1024]{1,0:T(8,128)(2,1)S(1)}, u32[]{:S(2)}, u32[]{:S(2)}) collective-permute-start(bf16[768,1024]{1,0:T(8,128)(2,1)} %bitcast.10), channel_id=1, source_target_pairs={{0,1},{1,0},{2,3},{3,2},{4,5},{5,4},{6,7},{7,6},{8,9},{9,8},{10,11... | collective-permute-start | bytes 4718600 | tf_op jit(solution)/shard_map/ppermute | solution.py:636
  3.2 4.0 %shard_map.127 = (f32[768,1024]{1,0:T(8,128)S(1)}, bf16[768,1024]{1,0:T(8,128)(2,1)S(1)}, f32[768,128]{1,0:T(8,128)S(1)}, f32[8,768]{1,0:T(8,128)S(1)}, f32[768,...) custom-call(s32[1]{0:T(128)} %bitcast.tp.side, bf16[768,1024]{1,0:T(8,128)(2,1)} %bitcast.11, ...), custom_call_target="tpu_custom_call" | custom-call | flops 1610612736 | bytes 1048576 | tf_op jit(solution)/shard_map/pallas_call | solution.py:184
  7.2 2.5 %shard_map.128 = (bf16[768,384]{1,0:T(8,128)(2,1)S(1)}, bf16[768,384]{1,0:T(8,128)(2,1)S(1)}, bf16[768,256]{1,0:T(8,128)(2,1)S(1)}, f32[768,128]{1,0:T(8,128)S(1...) custom-call(s32[1]{0:T(128)} %bitcast.tp.side, ...), custom_call_target="tpu_custom_call" | custom-call | flops 1610612736 | bytes 1048576 | tf_op jit(solution)/shard_map/pallas_call | solution.py:254
  9.7 1.1 %collective-permute-start.3 = (bf16[208,128]{1,0:T(8,128)(2,1)S(1)}, bf16[208,128]{1,0:T(8,128)(2,1)S(1)}, u32[]{:S(2)}, u32[]{:S(2)}) collective-permute-start(bf16[208,128]{1,0:T(8,128)(2,1)S(1)} %get-tuple-element.63.refs_0_), channel_id=1, source_target_pairs={{0,24},{8,0},{16,8},{24,16},{1,25},{9,1},{17,9},{25,17},{2,26},{10... | collective-permute-start | bytes 159752 | tf_op jit(solution)/shard_map/ppermute | solution.py:636
  10.8 0.3 collective-permute-start.2
  11.2 0.7 %collective-permute-start.1 = (bf16[208,128]{1,0:T(8,128)(2,1)S(1)}, bf16[208,128]{1,0:T(8,128)(2,1)S(1)}, u32[]{:S(2)}, u32[]{:S(2)}) collective-permute-start(bf16[208,128]{1,0:T(8,128)(2,1)S(1)} %get-tuple-element.63.refs_0_), channel_id=1, source_target_pairs={{0,8},{8,16},{16,24},{24,0},{1,9},{9,17},{17,25},{25,1},{2,10},{10... | collective-permute-start | bytes 159752 | tf_op jit(solution)/shard_map/ppermute | solution.py:636
  11.9 2.7 %shard_map.129 = (bf16[768,384]{1,0:T(8,128)(2,1)S(1)}, bf16[768,384]{1,0:T(8,128)(2,1)S(1)}) custom-call(s32[1]{0:T(128)} %bitcast.tp.side, bf16[768,1024]{1,0:T(8,128)(2,1)S(1)} %get-tuple-element.59.own, bf16[768,1024]{1,0:T(8,128)(2,1)S(1)} %get-tuple-element.60.peer, f32[768,128]{1,0:T(8,128)S(1)} %get-tuple-element.61.inv, ...), custom_call_target="tpu_custom_call" | custom-call | flops 2415919104 | bytes 1048576 | tf_op jit(solution)/shard_map/pallas_call | solution.py:290
  14.6 0.8 %collective-permute-done.2.refs_2_ = bf16[208,128]{1,0:T(8,128)(2,1)S(1)} collective-permute-done((bf16[208,128]{1,0:T(8,128)(2,1)S(1)}, bf16[208,128]{1,0:T(8,128)(2,1)S(1)}, u32[]{:S(2)}, u32[]{:S(2)}) %collective-permute-start.2) | collective-permute-done | bytes 53280 | tf_op jit(solution)/shard_map/ppermute | solution.py:636
  15.4 1.7 %collective-permute-done.1.refs_1_ = bf16[208,128]{1,0:T(8,128)(2,1)S(1)} collective-permute-done((bf16[208,128]{1,0:T(8,128)(2,1)S(1)}, bf16[208,128]{1,0:T(8,128)(2,1)S(1)}, u32[]{:S(2)}, u32[]{:S(2)}) %collective-permute-start.1) | collective-permute-done | bytes 53280 | tf_op jit(solution)/shard_map/ppermute | solution.py:636
  17.1 0.1 shard_map.130
  17.3 0.7 %collective-permute-start.10 = (bf16[384,2048]{1,0:T(8,128)(2,1)S(1)}, bf16[384,2048]{1,0:T(8,128)(2,1)S(1)}, u32[]{:S(2)}, u32[]{:S(2)}) collective-permute-start(bf16[384,2048]{1,0:T(8,128)(2,1)S(1)} %copy-done), channel_id=1, source_target_pairs={{0,1},{1,0},{2,3},{3,2},{4,5},{5,4},{6,7},{7,6},{8,9},{9,8},{10,11... | collective-permute-start | bytes 4718600 | tf_op jit(solution)/shard_map/ppermute | solution.py:636
  18.1 5.6 %collective-permute-start.5 = (bf16[208,128]{1,0:T(8,128)(2,1)S(1)}, bf16[208,128]{1,0:T(8,128)(2,1)S(1)}, u32[]{:S(2)}, u32[]{:S(2)}) collective-permute-start(bf16[208,128]{1,0:T(8,128)(2,1)S(1)} %get-tuple-element.75.own), channel_id=1, source_target_pairs={{0,224},{32,0},{64,32},{96,64},{128,96},{160,128},{192,160},{224,1... | collective-permute-start | bytes 159752 | tf_op jit(solution)/shard_map/ppermute | solution.py:636
  23.6 2.1 %collective-permute-done.6.halo_ref = bf16[128,256]{1,0:T(8,128)(2,1)S(1)} collective-permute-done((bf16[128,256]{1,0:T(8,128)(2,1)S(1)}, bf16[128,256]{1,0:T(8,128)(2,1)S(1)}, u32[]{:S(2)}, u32[]{:S(2)}) %collective-permute-start.6) | collective-permute-done | bytes 65568 | tf_op jit(solution)/shard_map/ppermute | solution.py:672
  25.7 2.6 %shard_map.131 = bf16[384,384]{1,0:T(8,128)(2,1)S(1)} custom-call(s32[1]{0:T(128)} %bitcast.tp.side, s32[1]{0:T(128)} %bitcast.1.spot, bf16[768,384]{1,0:T(8,128)(2,1)S(1)} %get-tuple-element.72.q_ref, bf16[768,256]{1,0:T(8,128)(2,1)S(1)} %get-tuple-element.73.kv_ref, bf16[128,256]{1,0:T(8,128)(2,1)S(1)} %collective-permute-done.6.halo_ref, f32[6]{0:T(128)S(1)} %copy-done.6), custom_call_target="tpu_custom_call" | custom-call | flops 1073741824 | bytes 1048576 | tf_op jit(solution)/shard_map/pallas_call | solution.py:548
  28.4 3.7 %collective-permute-start.8 = (bf16[208,128]{1,0:T(8,128)(2,1)S(1)}, bf16[208,128]{1,0:T(8,128)(2,1)S(1)}, u32[]{:S(2)}, u32[]{:S(2)}) collective-permute-start(bf16[208,128]{1,0:T(8,128)(2,1)S(1)} %get-tuple-element.78), channel_id=1, source_target_pairs={{0,192},{32,224},{64,0},{96,32},{128,64},{160,96},{192,128},{224,1... | collective-permute-start | bytes 159752 | tf_op jit(solution)/shard_map/ppermute | solution.py:636
  32.1 1.9 %collective-permute-start.9 = (bf16[384,384]{1,0:T(8,128)(2,1)S(1)}, bf16[384,384]{1,0:T(8,128)(2,1)S(1)}, u32[]{:S(2)}, u32[]{:S(2)}) collective-permute-start(bf16[384,384]{1,0:T(8,128)(2,1)S(1)} %shard_map.131), channel_id=1, source_target_pairs={{0,1},{1,0},{2,3},{3,2},{4,5},{5,4},{6,7},{7,6},{8,9},{9,8},{10,11... | collective-permute-start | bytes 884744 | tf_op jit(solution)/shard_map/ppermute | solution.py:636
  34.0 2.6 %shard_map.133.a = bf16[384,384]{1,0:T(8,128)(2,1)S(1)} custom-call(s32[1]{0:T(128)} %bitcast.tp.side, s32[1]{0:T(128)} %bitcast.1.spot, bf16[768,384]{1,0:T(8,128)(2,1)S(1)} %get-tuple-element.72.q_ref, bf16[768,256]{1,0:T(8,128)(2,1)S(1)} %get-tuple-element.73.kv_ref, bf16[128,256]{1,0:T(8,128)(2,1)S(1)} %collective-permute-done.6.halo_ref, f32[6]{0:T(128)S(1)} %copy-done.6), custom_call_target="tpu_custom_call" | custom-call | flops 1073741824 | bytes 1048576 | tf_op jit(solution)/shard_map/pallas_call | solution.py:548
  36.6 2.1 %shard_map.135.in_ref = f32[768,384]{1,0:T(8,128)S(1)} custom-call(bf16[768,384]{1,0:T(8,128)(2,1)S(1)} %get-tuple-element.83.q_ref, bf16[768,384]{1,0:T(8,128)(2,1)S(1)} %get-tuple-element.86.k_ref, bf16[768,384]{1,0:T(8,128)(2,1)S(1)} %get-tuple-element.87.v_ref, f32[8,768]{1,0:T(8,128)S(1)} %get-tuple-element.88.row_ref, ...), custom_call_target="tpu_custom_call" | custom-call | flops 3221225472 | bytes 1048576 | tf_op jit(solution)/shard_map/pallas_call | solution.py:343
  38.7 1.4 %shard_map.134.more = f32[384,2048]{1,0:T(8,128)S(1)} custom-call(bf16[384,384]{1,0:T(8,128)(2,1)S(1)} %shard_map.133.a, bf16[384,384]{1,0:T(8,128)(2,1)S(1)} %collective-permute-done.9.b, bf16[384,2048]{1,0:T(8,128)(2,1)S(1)} %copy-done, bf16[384,2048]{1,0:T(8,128)(2,1)S(1)} %collective-permute-done.10.wb), custom_call_target="tpu_custom_call" | custom-call | flops 1207959552 | bytes 1048576 | tf_op jit(solution)/shard_map/pallas_call | solution.py:593
  40.1 0.7 %shard_map.136 = bf16[384,384]{1,0:T(8,128)(2,1)S(1)} custom-call(s32[1]{0:T(128)} %bitcast.tp.side, s32[1]{0:T(128)} %bitcast.2.place.row, bf16[768,384]{1,0:T(8,128)(2,1)S(1)} %get-tuple-element.83.q_ref, f32[768,384]{1,0:T(8,128)S(1)} %shard_map.135.in_ref, f32[768,384]{1,0:T(8,128)S(1)} %get-tuple-element.56.col.col_ref, f32[384]{0:T(512)S(1)} %copy-done.2, ...), custom_call_target="tpu_custom_call" | custom-call | flops 536870912 | bytes 1048576 | tf_op jit(solution)/shard_map/pallas_call | solution.py:475
  40.8 1.7 %collective-permute-start.11 = (bf16[384,384]{1,0:T(8,128)(2,1)S(1)}, bf16[384,384]{1,0:T(8,128)(2,1)S(1)}, u32[]{:S(2)}, u32[]{:S(2)}) collective-permute-start(bf16[384,384]{1,0:T(8,128)(2,1)S(1)} %shard_map.136), channel_id=1, source_target_pairs={{0,1},{1,0},{2,3},{3,2},{4,5},{5,4},{6,7},{7,6},{8,9},{9,8},{10,11... | collective-permute-start | bytes 884744 | tf_op jit(solution)/shard_map/ppermute | solution.py:636
  42.4 0.7 %shard_map.137.a = bf16[384,384]{1,0:T(8,128)(2,1)S(1)} custom-call(s32[1]{0:T(128)} %bitcast.tp.side, s32[1]{0:T(128)} %bitcast.2.place.row, bf16[768,384]{1,0:T(8,128)(2,1)S(1)} %get-tuple-element.83.q_ref, f32[768,384]{1,0:T(8,128)S(1)} %shard_map.135.in_ref, f32[768,384]{1,0:T(8,128)S(1)} %get-tuple-element.56.col.col_ref, f32[384]{0:T(512)S(1)} %copy-done.2, ...), custom_call_target="tpu_custom_call" | custom-call | flops 536870912 | bytes 1048576 | tf_op jit(solution)/shard_map/pallas_call | solution.py:475
  43.1 1.0 %shard_map.138.more = f32[384,2048]{1,0:T(8,128)S(1)} custom-call(bf16[384,384]{1,0:T(8,128)(2,1)S(1)} %shard_map.137.a, bf16[384,2048]{1,0:T(8,128)(2,1)S(1)} %copy-done.1, f32[384,2048]{1,0:T(8,128)S(1)} %shard_map.134.more), custom_call_target="tpu_custom_call" | custom-call | flops 603979776 | bytes 1048576 | tf_op jit(solution)/shard_map/pallas_call | solution.py:607
  44.1 1.9 %shard_map.139 = bf16[384,2048]{1,0:T(8,128)(2,1)} custom-call(bf16[384,384]{1,0:T(8,128)(2,1)S(1)} %collective-permute-done.11.a, bf16[384,2048]{1,0:T(8,128)(2,1)S(1)} %collective-permute-done.12.w, f32[384,2048]{1,0:T(8,128)S(1)} %shard_map.138.more), custom_call_target="tpu_custom_call" | custom-call | flops 603979776 | bytes 1048576 | tf_op jit(solution)/shard_map/pallas_call | solution.py:622
  (29 shorter events, 0.2 us)
Async XLA Ops:
  0.0 7.2 %collective-permute-start = (bf16[768,1024]{1,0:T(8,128)(2,1)}, bf16[768,1024]{1,0:T(8,128)(2,1)S(1)}, u32[]{:S(2)}, u32[]{:S(2)}) collective-permute-start(bf16[768,1024]{1,0:T(8,128)(2,1)} %bitcast.10), channel_id=1, source_target_pairs={{0,1},{1,0},{2,3},{3,2},{4,5},{5,4},{6,7},{7,6},{8,9},{9,8},{10,11... | collective-permute-start | bytes 4718600 | tf_op jit(solution)/shard_map/ppermute | solution.py:636
  3.2 4.0 %copy-start.3 = (f32[2048]{0:T(1024)S(1)}, f32[2048]{0:T(1024)}, u32[]{:S(2)}) copy-start(f32[2048]{0:T(1024)} %param.14) | copy-start | bytes 24580
  7.2 4.7 %copy-start.4 = (bf16[2048,384]{1,0:T(8,128)(2,1)S(1)}, bf16[2048,384]{1,0:T(8,128)(2,1)}, u32[]{:S(2)}) copy-start(bf16[2048,384]{1,0:T(8,128)(2,1)} %w0.1) | copy-start | bytes 4718596
  7.2 4.7 %copy-start.5 = (bf16[2048,384]{1,0:T(8,128)(2,1)S(1)}, bf16[2048,384]{1,0:T(8,128)(2,1)}, u32[]{:S(2)}) copy-start(bf16[2048,384]{1,0:T(8,128)(2,1)} %w1.1) | copy-start | bytes 4718596
  9.7 4.8 %collective-permute-start.3 = (bf16[208,128]{1,0:T(8,128)(2,1)S(1)}, bf16[208,128]{1,0:T(8,128)(2,1)S(1)}, u32[]{:S(2)}, u32[]{:S(2)}) collective-permute-start(bf16[208,128]{1,0:T(8,128)(2,1)S(1)} %get-tuple-element.63.refs_0_), channel_id=1, source_target_pairs={{0,24},{8,0},{16,8},{24,16},{1,25},{9,1},{17,9},{25,17},{2,26},{10... | collective-permute-start | bytes 159752 | tf_op jit(solution)/shard_map/ppermute | solution.py:636
  10.8 4.5 %collective-permute-start.2 = (bf16[208,128]{1,0:T(8,128)(2,1)S(1)}, bf16[208,128]{1,0:T(8,128)(2,1)S(1)}, u32[]{:S(2)}, u32[]{:S(2)}) collective-permute-start(bf16[208,128]{1,0:T(8,128)(2,1)S(1)} %get-tuple-element.63.refs_0_), channel_id=1, source_target_pairs={{0,16},{8,24},{16,0},{24,8},{1,17},{9,25},{17,1},{25,9},{2,18},{10... | collective-permute-start | bytes 159752 | tf_op jit(solution)/shard_map/ppermute | solution.py:636
  11.2 5.9 %collective-permute-start.1 = (bf16[208,128]{1,0:T(8,128)(2,1)S(1)}, bf16[208,128]{1,0:T(8,128)(2,1)S(1)}, u32[]{:S(2)}, u32[]{:S(2)}) collective-permute-start(bf16[208,128]{1,0:T(8,128)(2,1)S(1)} %get-tuple-element.63.refs_0_), channel_id=1, source_target_pairs={{0,8},{8,16},{16,24},{24,0},{1,9},{9,17},{17,25},{25,1},{2,10},{10... | collective-permute-start | bytes 159752 | tf_op jit(solution)/shard_map/ppermute | solution.py:636
  11.9 5.4 %copy-start = (bf16[384,2048]{1,0:T(8,128)(2,1)S(1)}, bf16[384,2048]{1,0:T(8,128)(2,1)}, u32[]{:S(2)}) copy-start(bf16[384,2048]{1,0:T(8,128)(2,1)} %wa.1) | copy-start | bytes 4718596
  11.9 6.1 %copy-start.1 = (bf16[384,2048]{1,0:T(8,128)(2,1)S(1)}, bf16[384,2048]{1,0:T(8,128)(2,1)}, u32[]{:S(2)}) copy-start(bf16[384,2048]{1,0:T(8,128)(2,1)} %w.1) | copy-start | bytes 4718596
  11.9 13.8 %copy-start.6 = (f32[6]{0:T(128)S(1)}, f32[6]{0:T(128)}, u32[]{:S(2)}) copy-start(f32[6]{0:T(128)} %sink_ref.3) | copy-start | bytes 76
  17.3 21.4 %collective-permute-start.10 = (bf16[384,2048]{1,0:T(8,128)(2,1)S(1)}, bf16[384,2048]{1,0:T(8,128)(2,1)S(1)}, u32[]{:S(2)}, u32[]{:S(2)}) collective-permute-start(bf16[384,2048]{1,0:T(8,128)(2,1)S(1)} %copy-done), channel_id=1, source_target_pairs={{0,1},{1,0},{2,3},{3,2},{4,5},{5,4},{6,7},{7,6},{8,9},{9,8},{10,11... | collective-permute-start | bytes 4718600 | tf_op jit(solution)/shard_map/ppermute | solution.py:636
  18.0 26.2 %collective-permute-start.12 = (bf16[384,2048]{1,0:T(8,128)(2,1)S(1)}, bf16[384,2048]{1,0:T(8,128)(2,1)S(1)}, u32[]{:S(2)}, u32[]{:S(2)}) collective-permute-start(bf16[384,2048]{1,0:T(8,128)(2,1)S(1)} %copy-done.1), channel_id=1, source_target_pairs={{0,1},{1,0},{2,3},{3,2},{4,5},{5,4},{6,7},{7,6},{8,9},{9,8},{10,11... | collective-permute-start | bytes 4718600 | tf_op jit(solution)/shard_map/ppermute | solution.py:636
  18.1 7.6 %collective-permute-start.6 = (bf16[128,256]{1,0:T(8,128)(2,1)S(1)}, bf16[128,256]{1,0:T(8,128)(2,1)S(1)}, u32[]{:S(2)}, u32[]{:S(2)}) collective-permute-start(bf16[128,256]{1,0:T(8,128)(2,1)S(1)} %get-tuple-element.74), channel_id=1, source_target_pairs={{0,8},{8,16},{16,24},{24,32},{32,40},{40,48},{48,56},{56,64},{64,7... | collective-permute-start | bytes 196616 | tf_op jit(solution)/shard_map/ppermute | solution.py:672
  18.1 10.2 %collective-permute-start.5 = (bf16[208,128]{1,0:T(8,128)(2,1)S(1)}, bf16[208,128]{1,0:T(8,128)(2,1)S(1)}, u32[]{:S(2)}, u32[]{:S(2)}) collective-permute-start(bf16[208,128]{1,0:T(8,128)(2,1)S(1)} %get-tuple-element.75.own), channel_id=1, source_target_pairs={{0,224},{32,0},{64,32},{96,64},{128,96},{160,128},{192,160},{224,1... | collective-permute-start | bytes 159752 | tf_op jit(solution)/shard_map/ppermute | solution.py:636
  23.6 4.7 %collective-permute-start.4 = (bf16[208,128]{1,0:T(8,128)(2,1)S(1)}, bf16[208,128]{1,0:T(8,128)(2,1)S(1)}, u32[]{:S(2)}, u32[]{:S(2)}) collective-permute-start(bf16[208,128]{1,0:T(8,128)(2,1)S(1)} %get-tuple-element.75.own), channel_id=1, source_target_pairs={{0,32},{32,64},{64,96},{96,128},{128,160},{160,192},{192,224},{224... | collective-permute-start | bytes 159752 | tf_op jit(solution)/shard_map/ppermute | solution.py:636
  28.4 11.7 %collective-permute-start.8 = (bf16[208,128]{1,0:T(8,128)(2,1)S(1)}, bf16[208,128]{1,0:T(8,128)(2,1)S(1)}, u32[]{:S(2)}, u32[]{:S(2)}) collective-permute-start(bf16[208,128]{1,0:T(8,128)(2,1)S(1)} %get-tuple-element.78), channel_id=1, source_target_pairs={{0,192},{32,224},{64,0},{96,32},{128,64},{160,96},{192,128},{224,1... | collective-permute-start | bytes 159752 | tf_op jit(solution)/shard_map/ppermute | solution.py:636
  32.1 8.0 %collective-permute-start.7 = (bf16[208,128]{1,0:T(8,128)(2,1)S(1)}, bf16[208,128]{1,0:T(8,128)(2,1)S(1)}, u32[]{:S(2)}, u32[]{:S(2)}) collective-permute-start(bf16[208,128]{1,0:T(8,128)(2,1)S(1)} %get-tuple-element.78), channel_id=1, source_target_pairs={{0,96},{32,128},{64,160},{96,192},{128,224},{160,0},{192,32},{224,... | collective-permute-start | bytes 159752 | tf_op jit(solution)/shard_map/ppermute | solution.py:636
  32.1 6.6 %collective-permute-start.9 = (bf16[384,384]{1,0:T(8,128)(2,1)S(1)}, bf16[384,384]{1,0:T(8,128)(2,1)S(1)}, u32[]{:S(2)}, u32[]{:S(2)}) collective-permute-start(bf16[384,384]{1,0:T(8,128)(2,1)S(1)} %shard_map.131), channel_id=1, source_target_pairs={{0,1},{1,0},{2,3},{3,2},{4,5},{5,4},{6,7},{7,6},{8,9},{9,8},{10,11... | collective-permute-start | bytes 884744 | tf_op jit(solution)/shard_map/ppermute | solution.py:636
  38.6 1.5 %copy-start.2 = (f32[384]{0:T(512)S(1)}, f32[384]{0:T(512)}, u32[]{:S(2)}) copy-start(f32[384]{0:T(512)} %gain.3) | copy-start | bytes 4612
  40.8 3.3 %collective-permute-start.11 = (bf16[384,384]{1,0:T(8,128)(2,1)S(1)}, bf16[384,384]{1,0:T(8,128)(2,1)S(1)}, u32[]{:S(2)}, u32[]{:S(2)}) collective-permute-start(bf16[384,384]{1,0:T(8,128)(2,1)S(1)} %shard_map.136), channel_id=1, source_target_pairs={{0,1},{1,0},{2,3},{3,2},{4,5},{5,4},{6,7},{7,6},{8,9},{9,8},{10,11... | collective-permute-start | bytes 884744 | tf_op jit(solution)/shard_map/ppermute | solution.py:636

commit v2 on v1

--- a/solution.py
+++ b/solution.py
@@ -508,7 +508,9 @@
     band = (WINDOW, group * WINDOW)
     upper = row_ids(band) > lane_ids(band) % WINDOW
     empty = jnp.where((half == 0) & (first == 0), -jnp.inf, 0.0)
-    spot = lane_ids((1, group * WINDOW)) // WINDOW
+    levels = sink_ref[...].reshape(1, heads)
+    levels = [jnp.broadcast_to(levels[:, h : h + 1], (1, WINDOW)) for h in range(heads)]
+    sinks = [jnp.concatenate(levels[g * group : (g + 1) * group], axis=1) for g in range(2)]
     for block in range(rows // WINDOW):
         span = slice(block * WINDOW, (block + 2) * WINDOW)
         keys, values = ext[span, 0:LANES], ext[span, LANES:]
@@ -516,14 +518,13 @@
         outs = []
         for g in range(2):
             stack = []
-            sink = jnp.zeros((1, group * WINDOW), F32)
+            sink = sinks[g]
             for j in range(group):
                 h = g * group + j
                 q = q_ref[here, h // 2 * LANES : (h // 2 + 1) * LANES]
                 if h % 2 != g:
                     q = pltpu.roll(q.astype(F32), HEAD_DIM, 1).astype(BF16)
                 stack.append(q * masks[g])
-                sink = sink + jnp.where(spot == j, sink_ref[h], 0.0)
             scores = lax.dot_general(
                 keys, jnp.concatenate(stack, axis=0), CONTRACT_LANES, preferred_element_type=F32
             )
@@ -551,7 +552,7 @@
             pl.BlockSpec((rows // 2, width), lambda i, t, f: (half_of(t, mine), 0)),
             whole(kv.shape),
             whole(halo.shape),
-            pl.BlockSpec(memory_space=pltpu.SMEM),
+            whole(sinks.shape),
         ],
         whole((rows // 2, width)),
         jax.ShapeDtypeStruct((rows // 2, width), BF16),
@@ -602,18 +603,26 @@
     )(*args)
 
 
-def own_exit(a, w, more):
-    args = (a, w, more)
-    return call(
-        own_exit_body,
-        [whole(x.shape) for x in args],
+def finish_exit_body(side, row, q_ref, in_ref, col_ref, gain, *refs):
+    small, (w, more, out, rows) = refs[:6], refs[6:]
+    finish_body(side, row, q_ref, in_ref, col_ref, gain, *small, rows)
+    own_exit_body(rows, w, more, out)
+
+
+def finish_exit(side, row, q, inside, col, gain, small, w, more):
+    rows, width = q.shape
+    spec = pl.BlockSpec((rows // 2, width), lambda i, t, z: (half_of(t, True), 0))
+    rest = list(small) + [w, more]
+    return call(
+        finish_exit_body,
+        [spec, spec, spec, whole(gain.shape)] + [whole(s.shape) for s in rest],
         whole(more.shape),
         jax.ShapeDtypeStruct(more.shape, F32),
-        [],
-        0,
-        2 * a.shape[0] * a.shape[1] * w.shape[1],
-        12,
-    )(*args)
+        [pltpu.VMEM((rows // 2, width), BF16)],
+        2,
+        2**29,
+        16,
+    )(side, row, q, inside, col, gain, *rest)
 
 
 def last_exit(a, w, more):
@@ -694,8 +703,7 @@
     small = [line, line_log, column, column_log] + sources
     args = (side, row, ret_q, inside, col, ret_gain, small)
     ret_got = turned(finish(False, *args), "tp", 1)
-    ret_mine = finish(True, *args)
-    partial = own_exit(ret_mine, retentive_exit_matrix, partial)
+    partial = finish_exit(*args, retentive_exit_matrix, partial)
     mixed = last_exit(ret_got, exit_peer, partial)
     return mixed[None]
 

time: 46.3 us -> 45 us (0.972)
  Pallas kernels: 22.2 us -> 20.9 us
    pallas_call x2, Pallas kernels: 5.16 us -> 4.07 us  [window(): call(functools.partial(window_body, mine), [pl.BlockSpec((rows // 2, widt...]
    pallas_call x2 -> x1, Pallas kernels: 1.31 us -> 0.66 us  [finish(): call(finish_body, [spec, spec, spec, whole(gain.shape)] + [whole(s.shape)...]
    pallas_call x1, Pallas kernels: 1.02 us -> 1.52 us  [finish_exit(): call(finish_exit_body, [spec, spec, spec, whole(gain.shape)] + [whole(s.s...]
  transfers between devices with their start and end apart: 13 -> 13, of which waited for: 3 -> 4; matrix products, arithmetic and copies ran while one was open for 0% -> 0% of each run, Pallas kernels for 38% -> 36%
where the time goes in v2:
time: 45 us
  Pallas kernels  20.9 us (46%)
  starting transfers between devices  19 us (42%)
  waiting for transfers between devices  4.69 us (10%)
    ppermute x12, starting transfers between devices, turned(): lax.ppermute(value, axis, [(i, (i + by) % peers) for i in range(peers)])  19 us
    pallas_call x2, Pallas kernels, window(): call(functools.partial(window_body, mine), [pl.BlockSpec((rows // 2, widt...  4.07 us
    pallas_call x1, Pallas kernels, own_half(): call(own_body, [IN_HBM] * 7, [whole(s) for s, _ in shapes], [jax.ShapeDty...  3.96 us
    pallas_call x1, Pallas kernels, queries(): call(queries_body, [whole(a.shape) for a in (own, peer, inv, w0, w1)], [w...  2.67 us
    ppermute x12, waiting for transfers between devices, turned(): lax.ppermute(value, axis, [(i, (i + by) % peers) for i in range(peers)])  2.63 us
    pallas_call x1, Pallas kernels, keys_half(): call(keys_body, [whole(a.shape) for a in (peer, gain, part, sq, col, wbuf...  2.5 us
    ppermute x1, waiting for transfers between devices, shards(): halo = lax.ppermute(tail, SP, [(i, (i + 1) % peers) for i in range(peers)])  2.06 us
    pallas_call x1, Pallas kernels, inner(): call(inner_body, [whole(a.shape) for a in args], whole(q.shape), jax.Shap...  2.04 us
  transfers between devices with their start and end apart: 13, of which 4 were waited for; matrix products, arithmetic and copies ran while one was open for 0% of the time, Pallas kernels for 36%

profile of v2, /device:TPU:1, one launch (start us, length us, event | category | flops | bytes accessed | tf_op | source)
XLA Modules:
  0.0 45.0 jit_solution(2385032287539207879)
XLA Ops:
  0.0 3.2 %collective-permute-start = (bf16[768,1024]{1,0:T(8,128)(2,1)}, bf16[768,1024]{1,0:T(8,128)(2,1)S(1)}, u32[]{:S(2)}, u32[]{:S(2)}) collective-permute-start(bf16[768,1024]{1,0:T(8,128)(2,1)} %bitcast.10), channel_id=1, source_target_pairs={{0,1},{1,0},{2,3},{3,2},{4,5},{5,4},{6,7},{7,6},{8,9},{9,8},{10,11... | collective-permute-start | bytes 4718600 | tf_op jit(solution)/shard_map/ppermute | solution.py:645
  3.2 4.0 %shard_map.127 = (f32[768,1024]{1,0:T(8,128)S(1)}, bf16[768,1024]{1,0:T(8,128)(2,1)S(1)}, f32[768,128]{1,0:T(8,128)S(1)}, f32[8,768]{1,0:T(8,128)S(1)}, f32[768,...) custom-call(s32[1]{0:T(128)} %bitcast.tp.side, bf16[768,1024]{1,0:T(8,128)(2,1)} %bitcast.11, ...), custom_call_target="tpu_custom_call" | custom-call | flops 1610612736 | bytes 1048576 | tf_op jit(solution)/shard_map/pallas_call | solution.py:184
  7.2 2.5 %shard_map.128 = (bf16[768,384]{1,0:T(8,128)(2,1)S(1)}, bf16[768,384]{1,0:T(8,128)(2,1)S(1)}, bf16[768,256]{1,0:T(8,128)(2,1)S(1)}, f32[768,128]{1,0:T(8,128)S(1...) custom-call(s32[1]{0:T(128)} %bitcast.tp.side, ...), custom_call_target="tpu_custom_call" | custom-call | flops 1610612736 | bytes 1048576 | tf_op jit(solution)/shard_map/pallas_call | solution.py:254
  9.7 1.1 %collective-permute-start.3 = (bf16[208,128]{1,0:T(8,128)(2,1)S(1)}, bf16[208,128]{1,0:T(8,128)(2,1)S(1)}, u32[]{:S(2)}, u32[]{:S(2)}) collective-permute-start(bf16[208,128]{1,0:T(8,128)(2,1)S(1)} %get-tuple-element.63.refs_0_), channel_id=1, source_target_pairs={{0,24},{8,0},{16,8},{24,16},{1,25},{9,1},{17,9},{25,17},{2,26},{10... | collective-permute-start | bytes 159752 | tf_op jit(solution)/shard_map/ppermute | solution.py:645
  10.8 0.3 collective-permute-start.2
  11.2 0.7 %collective-permute-start.1 = (bf16[208,128]{1,0:T(8,128)(2,1)S(1)}, bf16[208,128]{1,0:T(8,128)(2,1)S(1)}, u32[]{:S(2)}, u32[]{:S(2)}) collective-permute-start(bf16[208,128]{1,0:T(8,128)(2,1)S(1)} %get-tuple-element.63.refs_0_), channel_id=1, source_target_pairs={{0,8},{8,16},{16,24},{24,0},{1,9},{9,17},{17,25},{25,1},{2,10},{10... | collective-permute-start | bytes 159752 | tf_op jit(solution)/shard_map/ppermute | solution.py:645
  11.9 2.7 %shard_map.129 = (bf16[768,384]{1,0:T(8,128)(2,1)S(1)}, bf16[768,384]{1,0:T(8,128)(2,1)S(1)}) custom-call(s32[1]{0:T(128)} %bitcast.tp.side, bf16[768,1024]{1,0:T(8,128)(2,1)S(1)} %get-tuple-element.59.own, bf16[768,1024]{1,0:T(8,128)(2,1)S(1)} %get-tuple-element.60.peer, f32[768,128]{1,0:T(8,128)S(1)} %get-tuple-element.61.inv, ...), custom_call_target="tpu_custom_call" | custom-call | flops 2415919104 | bytes 1048576 | tf_op jit(solution)/shard_map/pallas_call | solution.py:290
  14.6 0.8 %collective-permute-done.2.refs_2_ = bf16[208,128]{1,0:T(8,128)(2,1)S(1)} collective-permute-done((bf16[208,128]{1,0:T(8,128)(2,1)S(1)}, bf16[208,128]{1,0:T(8,128)(2,1)S(1)}, u32[]{:S(2)}, u32[]{:S(2)}) %collective-permute-start.2) | collective-permute-done | bytes 53280 | tf_op jit(solution)/shard_map/ppermute | solution.py:645
  15.4 1.7 %collective-permute-done.1.refs_1_ = bf16[208,128]{1,0:T(8,128)(2,1)S(1)} collective-permute-done((bf16[208,128]{1,0:T(8,128)(2,1)S(1)}, bf16[208,128]{1,0:T(8,128)(2,1)S(1)}, u32[]{:S(2)}, u32[]{:S(2)}) %collective-permute-start.1) | collective-permute-done | bytes 53280 | tf_op jit(solution)/shard_map/ppermute | solution.py:645
  17.1 0.1 shard_map.130
  17.2 0.7 %collective-permute-start.10 = (bf16[384,2048]{1,0:T(8,128)(2,1)S(1)}, bf16[384,2048]{1,0:T(8,128)(2,1)S(1)}, u32[]{:S(2)}, u32[]{:S(2)}) collective-permute-start(bf16[384,2048]{1,0:T(8,128)(2,1)S(1)} %copy-done.1), channel_id=1, source_target_pairs={{0,1},{1,0},{2,3},{3,2},{4,5},{5,4},{6,7},{7,6},{8,9},{9,8},{10,11... | collective-permute-start | bytes 4718600 | tf_op jit(solution)/shard_map/ppermute | solution.py:645
  17.9 0.1 collective-permute-start.12
  18.0 5.6 %collective-permute-start.5 = (bf16[208,128]{1,0:T(8,128)(2,1)S(1)}, bf16[208,128]{1,0:T(8,128)(2,1)S(1)}, u32[]{:S(2)}, u32[]{:S(2)}) collective-permute-start(bf16[208,128]{1,0:T(8,128)(2,1)S(1)} %get-tuple-element.75.own), channel_id=1, source_target_pairs={{0,224},{32,0},{64,32},{96,64},{128,96},{160,128},{192,160},{224,1... | collective-permute-start | bytes 159752 | tf_op jit(solution)/shard_map/ppermute | solution.py:645
  23.6 2.1 %collective-permute-done.6.halo_ref = bf16[128,256]{1,0:T(8,128)(2,1)S(1)} collective-permute-done((bf16[128,256]{1,0:T(8,128)(2,1)S(1)}, bf16[128,256]{1,0:T(8,128)(2,1)S(1)}, u32[]{:S(2)}, u32[]{:S(2)}) %collective-permute-start.6) | collective-permute-done | bytes 65568 | tf_op jit(solution)/shard_map/ppermute | solution.py:681
  25.7 2.0 %shard_map.131 = bf16[384,384]{1,0:T(8,128)(2,1)S(1)} custom-call(s32[1]{0:T(128)} %bitcast.tp.side, s32[1]{0:T(128)} %bitcast.1.spot, bf16[768,384]{1,0:T(8,128)(2,1)S(1)} %get-tuple-element.72.q_ref, bf16[768,256]{1,0:T(8,128)(2,1)S(1)} %get-tuple-element.73.kv_ref, bf16[128,256]{1,0:T(8,128)(2,1)S(1)} %collective-permute-done.6.halo_ref, f32[6]{0:T(128)S(1)} %copy-done.6), custom_call_target="tpu_custom_call" | custom-call | flops 1073741824 | bytes 1048576 | tf_op jit(solution)/shard_map/pallas_call | solution.py:549
  27.9 3.6 %collective-permute-start.8 = (bf16[208,128]{1,0:T(8,128)(2,1)S(1)}, bf16[208,128]{1,0:T(8,128)(2,1)S(1)}, u32[]{:S(2)}, u32[]{:S(2)}) collective-permute-start(bf16[208,128]{1,0:T(8,128)(2,1)S(1)} %get-tuple-element.78), channel_id=1, source_target_pairs={{0,192},{32,224},{64,0},{96,32},{128,64},{160,96},{192,128},{224,1... | collective-permute-start | bytes 159752 | tf_op jit(solution)/shard_map/ppermute | solution.py:645
  31.5 1.9 %collective-permute-start.9 = (bf16[384,384]{1,0:T(8,128)(2,1)S(1)}, bf16[384,384]{1,0:T(8,128)(2,1)S(1)}, u32[]{:S(2)}, u32[]{:S(2)}) collective-permute-start(bf16[384,384]{1,0:T(8,128)(2,1)S(1)} %shard_map.131), channel_id=1, source_target_pairs={{0,1},{1,0},{2,3},{3,2},{4,5},{5,4},{6,7},{7,6},{8,9},{9,8},{10,11... | collective-permute-start | bytes 884744 | tf_op jit(solution)/shard_map/ppermute | solution.py:645
  33.4 2.0 %shard_map.133.a = bf16[384,384]{1,0:T(8,128)(2,1)S(1)} custom-call(s32[1]{0:T(128)} %bitcast.tp.side, s32[1]{0:T(128)} %bitcast.1.spot, bf16[768,384]{1,0:T(8,128)(2,1)S(1)} %get-tuple-element.72.q_ref, bf16[768,256]{1,0:T(8,128)(2,1)S(1)} %get-tuple-element.73.kv_ref, bf16[128,256]{1,0:T(8,128)(2,1)S(1)} %collective-permute-done.6.halo_ref, f32[6]{0:T(128)S(1)} %copy-done.6), custom_call_target="tpu_custom_call" | custom-call | flops 1073741824 | bytes 1048576 | tf_op jit(solution)/shard_map/pallas_call | solution.py:549
  35.5 2.0 %shard_map.135.in_ref = f32[768,384]{1,0:T(8,128)S(1)} custom-call(bf16[768,384]{1,0:T(8,128)(2,1)S(1)} %get-tuple-element.83.q_ref, bf16[768,384]{1,0:T(8,128)(2,1)S(1)} %get-tuple-element.86.k_ref, bf16[768,384]{1,0:T(8,128)(2,1)S(1)} %get-tuple-element.87.v_ref, f32[8,768]{1,0:T(8,128)S(1)} %get-tuple-element.88.row_ref, ...), custom_call_target="tpu_custom_call" | custom-call | flops 3221225472 | bytes 1048576 | tf_op jit(solution)/shard_map/pallas_call | solution.py:343
  37.6 1.4 %shard_map.134.refs_7_ = f32[384,2048]{1,0:T(8,128)S(1)} custom-call(bf16[384,384]{1,0:T(8,128)(2,1)S(1)} %shard_map.133.a, bf16[384,384]{1,0:T(8,128)(2,1)S(1)} %collective-permute-done.9.b, bf16[384,2048]{1,0:T(8,128)(2,1)S(1)} %copy-done.1, bf16[384,2048]{1,0:T(8,128)(2,1)S(1)} %collective-permute-done.10.wb), custom_call_target="tpu_custom_call" | custom-call | flops 1207959552 | bytes 1048576 | tf_op jit(solution)/shard_map/pallas_call | solution.py:594
  39.0 0.7 %shard_map.136 = bf16[384,384]{1,0:T(8,128)(2,1)S(1)} custom-call(s32[1]{0:T(128)} %bitcast.tp.side, s32[1]{0:T(128)} %bitcast.2.place.row, bf16[768,384]{1,0:T(8,128)(2,1)S(1)} %get-tuple-element.83.q_ref, f32[768,384]{1,0:T(8,128)S(1)} %shard_map.135.in_ref, f32[768,384]{1,0:T(8,128)S(1)} %get-tuple-element.56.col.col_ref, f32[384]{0:T(512)S(1)} %copy-done.2, ...), custom_call_target="tpu_custom_call" | custom-call | flops 536870912 | bytes 1048576 | tf_op jit(solution)/shard_map/pallas_call | solution.py:475
  39.7 1.7 %collective-permute-start.11 = (bf16[384,384]{1,0:T(8,128)(2,1)S(1)}, bf16[384,384]{1,0:T(8,128)(2,1)S(1)}, u32[]{:S(2)}, u32[]{:S(2)}) collective-permute-start(bf16[384,384]{1,0:T(8,128)(2,1)S(1)} %shard_map.136), channel_id=1, source_target_pairs={{0,1},{1,0},{2,3},{3,2},{4,5},{5,4},{6,7},{7,6},{8,9},{9,8},{10,11... | collective-permute-start | bytes 884744 | tf_op jit(solution)/shard_map/ppermute | solution.py:645
  41.3 1.5 %shard_map.137.more = f32[384,2048]{1,0:T(8,128)S(1)} custom-call(s32[1]{0:T(128)} %bitcast.tp.side, s32[1]{0:T(128)} %bitcast.2.place.row, bf16[768,384]{1,0:T(8,128)(2,1)S(1)} %get-tuple-element.83.q_ref, f32[768,384]{1,0:T(8,128)S(1)} %shard_map.135.in_ref, f32[768,384]{1,0:T(8,128)S(1)} %get-tuple-element.56.col.col_ref, f32[384]{0:T(512)S(1)} %copy-done.2, ...), custom_call_target="tpu_custom_call" | custom-call | flops 536870912 | bytes 1048576 | tf_op jit(solution)/shard_map/pallas_call | solution.py:616
  42.9 1.9 %shard_map.138 = bf16[384,2048]{1,0:T(8,128)(2,1)} custom-call(bf16[384,384]{1,0:T(8,128)(2,1)S(1)} %collective-permute-done.11.a, bf16[384,2048]{1,0:T(8,128)(2,1)S(1)} %collective-permute-done.12.w, f32[384,2048]{1,0:T(8,128)S(1)} %shard_map.137.more), custom_call_target="tpu_custom_call" | custom-call | flops 603979776 | bytes 1048576 | tf_op jit(solution)/shard_map/pallas_call | solution.py:631
  (28 shorter events, 0.2 us)
Async XLA Ops:
  0.0 7.2 %collective-permute-start = (bf16[768,1024]{1,0:T(8,128)(2,1)}, bf16[768,1024]{1,0:T(8,128)(2,1)S(1)}, u32[]{:S(2)}, u32[]{:S(2)}) collective-permute-start(bf16[768,1024]{1,0:T(8,128)(2,1)} %bitcast.10), channel_id=1, source_target_pairs={{0,1},{1,0},{2,3},{3,2},{4,5},{5,4},{6,7},{7,6},{8,9},{9,8},{10,11... | collective-permute-start | bytes 4718600 | tf_op jit(solution)/shard_map/ppermute | solution.py:645
  3.2 4.0 %copy-start.3 = (f32[2048]{0:T(1024)S(1)}, f32[2048]{0:T(1024)}, u32[]{:S(2)}) copy-start(f32[2048]{0:T(1024)} %param.14) | copy-start | bytes 24580
  7.2 4.7 %copy-start.4 = (bf16[2048,384]{1,0:T(8,128)(2,1)S(1)}, bf16[2048,384]{1,0:T(8,128)(2,1)}, u32[]{:S(2)}) copy-start(bf16[2048,384]{1,0:T(8,128)(2,1)} %w0.1) | copy-start | bytes 4718596
  7.2 4.7 %copy-start.5 = (bf16[2048,384]{1,0:T(8,128)(2,1)S(1)}, bf16[2048,384]{1,0:T(8,128)(2,1)}, u32[]{:S(2)}) copy-start(bf16[2048,384]{1,0:T(8,128)(2,1)} %w1.1) | copy-start | bytes 4718596
  9.7 4.8 %collective-permute-start.3 = (bf16[208,128]{1,0:T(8,128)(2,1)S(1)}, bf16[208,128]{1,0:T(8,128)(2,1)S(1)}, u32[]{:S(2)}, u32[]{:S(2)}) collective-permute-start(bf16[208,128]{1,0:T(8,128)(2,1)S(1)} %get-tuple-element.63.refs_0_), channel_id=1, source_target_pairs={{0,24},{8,0},{16,8},{24,16},{1,25},{9,1},{17,9},{25,17},{2,26},{10... | collective-permute-start | bytes 159752 | tf_op jit(solution)/shard_map/ppermute | solution.py:645
  10.8 4.5 %collective-permute-start.2 = (bf16[208,128]{1,0:T(8,128)(2,1)S(1)}, bf16[208,128]{1,0:T(8,128)(2,1)S(1)}, u32[]{:S(2)}, u32[]{:S(2)}) collective-permute-start(bf16[208,128]{1,0:T(8,128)(2,1)S(1)} %get-tuple-element.63.refs_0_), channel_id=1, source_target_pairs={{0,16},{8,24},{16,0},{24,8},{1,17},{9,25},{17,1},{25,9},{2,18},{10... | collective-permute-start | bytes 159752 | tf_op jit(solution)/shard_map/ppermute | solution.py:645
  11.2 5.9 %collective-permute-start.1 = (bf16[208,128]{1,0:T(8,128)(2,1)S(1)}, bf16[208,128]{1,0:T(8,128)(2,1)S(1)}, u32[]{:S(2)}, u32[]{:S(2)}) collective-permute-start(bf16[208,128]{1,0:T(8,128)(2,1)S(1)} %get-tuple-element.63.refs_0_), channel_id=1, source_target_pairs={{0,8},{8,16},{16,24},{24,0},{1,9},{9,17},{17,25},{25,1},{2,10},{10... | collective-permute-start | bytes 159752 | tf_op jit(solution)/shard_map/ppermute | solution.py:645
  11.9 5.4 %copy-start.1 = (bf16[384,2048]{1,0:T(8,128)(2,1)S(1)}, bf16[384,2048]{1,0:T(8,128)(2,1)}, u32[]{:S(2)}) copy-start(bf16[384,2048]{1,0:T(8,128)(2,1)} %wa.1) | copy-start | bytes 4718596
  11.9 6.1 %copy-start = (bf16[384,2048]{1,0:T(8,128)(2,1)S(1)}, bf16[384,2048]{1,0:T(8,128)(2,1)}, u32[]{:S(2)}) copy-start(bf16[384,2048]{1,0:T(8,128)(2,1)} %refs_6_.1) | copy-start | bytes 4718596
  11.9 13.8 %copy-start.6 = (f32[6]{0:T(128)S(1)}, f32[6]{0:T(128)}, u32[]{:S(2)}) copy-start(f32[6]{0:T(128)} %sink_ref.3) | copy-start | bytes 76
  17.2 20.3 %collective-permute-start.10 = (bf16[384,2048]{1,0:T(8,128)(2,1)S(1)}, bf16[384,2048]{1,0:T(8,128)(2,1)S(1)}, u32[]{:S(2)}, u32[]{:S(2)}) collective-permute-start(bf16[384,2048]{1,0:T(8,128)(2,1)S(1)} %copy-done.1), channel_id=1, source_target_pairs={{0,1},{1,0},{2,3},{3,2},{4,5},{5,4},{6,7},{7,6},{8,9},{9,8},{10,11... | collective-permute-start | bytes 4718600 | tf_op jit(solution)/shard_map/ppermute | solution.py:645
  17.9 24.9 %collective-permute-start.12 = (bf16[384,2048]{1,0:T(8,128)(2,1)S(1)}, bf16[384,2048]{1,0:T(8,128)(2,1)S(1)}, u32[]{:S(2)}, u32[]{:S(2)}) collective-permute-start(bf16[384,2048]{1,0:T(8,128)(2,1)S(1)} %copy-done), channel_id=1, source_target_pairs={{0,1},{1,0},{2,3},{3,2},{4,5},{5,4},{6,7},{7,6},{8,9},{9,8},{10,11... | collective-permute-start | bytes 4718600 | tf_op jit(solution)/shard_map/ppermute | solution.py:645
  18.0 7.6 %collective-permute-start.6 = (bf16[128,256]{1,0:T(8,128)(2,1)S(1)}, bf16[128,256]{1,0:T(8,128)(2,1)S(1)}, u32[]{:S(2)}, u32[]{:S(2)}) collective-permute-start(bf16[128,256]{1,0:T(8,128)(2,1)S(1)} %get-tuple-element.74), channel_id=1, source_target_pairs={{0,8},{8,16},{16,24},{24,32},{32,40},{40,48},{48,56},{56,64},{64,7... | collective-permute-start | bytes 196616 | tf_op jit(solution)/shard_map/ppermute | solution.py:681
  18.0 9.7 %collective-permute-start.5 = (bf16[208,128]{1,0:T(8,128)(2,1)S(1)}, bf16[208,128]{1,0:T(8,128)(2,1)S(1)}, u32[]{:S(2)}, u32[]{:S(2)}) collective-permute-start(bf16[208,128]{1,0:T(8,128)(2,1)S(1)} %get-tuple-element.75.own), channel_id=1, source_target_pairs={{0,224},{32,0},{64,32},{96,64},{128,96},{160,128},{192,160},{224,1... | collective-permute-start | bytes 159752 | tf_op jit(solution)/shard_map/ppermute | solution.py:645
  23.6 4.2 %collective-permute-start.4 = (bf16[208,128]{1,0:T(8,128)(2,1)S(1)}, bf16[208,128]{1,0:T(8,128)(2,1)S(1)}, u32[]{:S(2)}, u32[]{:S(2)}) collective-permute-start(bf16[208,128]{1,0:T(8,128)(2,1)S(1)} %get-tuple-element.75.own), channel_id=1, source_target_pairs={{0,32},{32,64},{64,96},{96,128},{128,160},{160,192},{192,224},{224... | collective-permute-start | bytes 159752 | tf_op jit(solution)/shard_map/ppermute | solution.py:645
  27.9 11.1 %collective-permute-start.8 = (bf16[208,128]{1,0:T(8,128)(2,1)S(1)}, bf16[208,128]{1,0:T(8,128)(2,1)S(1)}, u32[]{:S(2)}, u32[]{:S(2)}) collective-permute-start(bf16[208,128]{1,0:T(8,128)(2,1)S(1)} %get-tuple-element.78), channel_id=1, source_target_pairs={{0,192},{32,224},{64,0},{96,32},{128,64},{160,96},{192,128},{224,1... | collective-permute-start | bytes 159752 | tf_op jit(solution)/shard_map/ppermute | solution.py:645
  31.5 7.5 %collective-permute-start.7 = (bf16[208,128]{1,0:T(8,128)(2,1)S(1)}, bf16[208,128]{1,0:T(8,128)(2,1)S(1)}, u32[]{:S(2)}, u32[]{:S(2)}) collective-permute-start(bf16[208,128]{1,0:T(8,128)(2,1)S(1)} %get-tuple-element.78), channel_id=1, source_target_pairs={{0,96},{32,128},{64,160},{96,192},{128,224},{160,0},{192,32},{224,... | collective-permute-start | bytes 159752 | tf_op jit(solution)/shard_map/ppermute | solution.py:645
  31.5 6.0 %collective-permute-start.9 = (bf16[384,384]{1,0:T(8,128)(2,1)S(1)}, bf16[384,384]{1,0:T(8,128)(2,1)S(1)}, u32[]{:S(2)}, u32[]{:S(2)}) collective-permute-start(bf16[384,384]{1,0:T(8,128)(2,1)S(1)} %shard_map.131), channel_id=1, source_target_pairs={{0,1},{1,0},{2,3},{3,2},{4,5},{5,4},{6,7},{7,6},{8,9},{9,8},{10,11... | collective-permute-start | bytes 884744 | tf_op jit(solution)/shard_map/ppermute | solution.py:645
  37.5 1.5 %copy-start.2 = (f32[384]{0:T(512)S(1)}, f32[384]{0:T(512)}, u32[]{:S(2)}) copy-start(f32[384]{0:T(512)} %gain.3) | copy-start | bytes 4612
  39.7 3.2 %collective-permute-start.11 = (bf16[384,384]{1,0:T(8,128)(2,1)S(1)}, bf16[384,384]{1,0:T(8,128)(2,1)S(1)}, u32[]{:S(2)}, u32[]{:S(2)}) collective-permute-start(bf16[384,384]{1,0:T(8,128)(2,1)S(1)} %shard_map.136), channel_id=1, source_target_pairs={{0,1},{1,0},{2,3},{3,2},{4,5},{5,4},{6,7},{7,6},{8,9},{9,8},{10,11... | collective-permute-start | bytes 884744 | tf_op jit(solution)/shard_map/ppermute | solution.py:645

commit v3 on v2

--- a/solution.py
+++ b/solution.py
@@ -676,7 +676,10 @@
     ret_k, ret_v, att_kv, inv, scaled, payload, tail = keys_half(
         side, peer, gain, first, squares, col, late, ret_key.shape[1]
     )
-    sources = [payload] + [turned(payload, "sp_1", k) for k in (1, 2, 3)]
+    hops = {}
+    for k in (1, 2, 3):
+        hops[k] = turned(payload, "sp_1", k)
+    sources = [payload] + [hops[k] for k in (1, 2, 3)]
     peers = lax.axis_size(SP)
     halo = lax.ppermute(tail, SP, [(i, (i + 1) % peers) for i in range(peers)])
     ret_q, att_q = queries(side, scaled_own, scaled, inv, ret_query, att_query)
@@ -690,10 +693,12 @@
     )
     out_peer = turned(out_own, "tp", 1)
     exit_peer = turned(exit_own, "tp", 1)
+    att_got = turned(theirs, "tp", 1)
     sources, theirs = lax.optimization_barrier((sources, theirs))
-    att_got = turned(theirs, "tp", 1)
     column, column_log, span = scan_step(column_body, row, sources)
-    sources = [turned(span, "sp_0", 3), turned(span, "sp_0", 6)]
+    three = turned(span, "sp_0", 3)
+    six = turned(span, "sp_0", 6)
+    sources = [three, six]
     side, row, span = lax.optimization_barrier((side, row, span))
     att_mine = window(True, side, spot, att_q, att_kv, halo, sink_logit)
     ret_q, row = lax.optimization_barrier((ret_q, row))

time: 45 us -> 45.4 us (level)
  waiting for transfers between devices: 4.69 us -> 6.04 us
  starting transfers between devices: 19 us -> 18 us
    ppermute x12, waiting for transfers between devices: 2.63 us -> 3.99 us  [turned(): lax.ppermute(value, axis, [(i, (i + by) % peers) for i in range(peers)])]
    ppermute x12, starting transfers between devices: 19 us -> 18 us  [turned(): lax.ppermute(value, axis, [(i, (i + by) % peers) for i in range(peers)])]
where the time goes in v3:
time: 45.4 us; the launch traced here: 45.3 us
  Pallas kernels  20.9 us (46%)
  starting transfers between devices  18 us (40%)
  waiting for transfers between devices  6.04 us (13%)
    ppermute x12, starting transfers between devices, turned(): lax.ppermute(value, axis, [(i, (i + by) % peers) for i in range(peers)])  18 us
    pallas_call x2, Pallas kernels, window(): call(functools.partial(window_body, mine), [pl.BlockSpec((rows // 2, widt...  4.08 us
    ppermute x12, waiting for transfers between devices, turned(): lax.ppermute(value, axis, [(i, (i + by) % peers) for i in range(peers)])  3.99 us
    pallas_call x1, Pallas kernels, own_half(): call(own_body, [IN_HBM] * 7, [whole(s) for s, _ in shapes], [jax.ShapeDty...  3.96 us
    pallas_call x1, Pallas kernels, queries(): call(queries_body, [whole(a.shape) for a in (own, peer, inv, w0, w1)], [w...  2.67 us
    pallas_call x1, Pallas kernels, keys_half(): call(keys_body, [whole(a.shape) for a in (peer, gain, part, sq, col, wbuf...  2.5 us
    ppermute x1, waiting for transfers between devices, shards(): halo = lax.ppermute(tail, SP, [(i, (i + 1) % peers) for i in range(peers)])  2.06 us
    pallas_call x1, Pallas kernels, inner(): call(inner_body, [whole(a.shape) for a in args], whole(q.shape), jax.Shap...  2.04 us
  transfers between devices with their start and end apart: 13, of which 4 were waited for; matrix products, arithmetic and copies ran while one was open for 0% of the time, Pallas kernels for 36%

profile of v3, /device:TPU:1, one launch (start us, length us, event | category | flops | bytes accessed | tf_op | source)
XLA Modules:
  0.0 45.3 jit_solution(4363989229146702138)
XLA Ops:
  0.0 3.2 %collective-permute-start = (bf16[768,1024]{1,0:T(8,128)(2,1)}, bf16[768,1024]{1,0:T(8,128)(2,1)S(1)}, u32[]{:S(2)}, u32[]{:S(2)}) collective-permute-start(bf16[768,1024]{1,0:T(8,128)(2,1)} %bitcast.10), channel_id=1, source_target_pairs={{0,1},{1,0},{2,3},{3,2},{4,5},{5,4},{6,7},{7,6},{8,9},{9,8},{10,11... | collective-permute-start | bytes 4718600 | tf_op jit(solution)/shard_map/ppermute | solution.py:645
  3.2 4.0 %shard_map.127 = (f32[768,1024]{1,0:T(8,128)S(1)}, bf16[768,1024]{1,0:T(8,128)(2,1)S(1)}, f32[768,128]{1,0:T(8,128)S(1)}, f32[8,768]{1,0:T(8,128)S(1)}, f32[768,...) custom-call(s32[1]{0:T(128)} %bitcast.tp.side, bf16[768,1024]{1,0:T(8,128)(2,1)} %bitcast.11, ...), custom_call_target="tpu_custom_call" | custom-call | flops 1610612736 | bytes 1048576 | tf_op jit(solution)/shard_map/pallas_call | solution.py:184
  7.2 2.5 %shard_map.128 = (bf16[768,384]{1,0:T(8,128)(2,1)S(1)}, bf16[768,384]{1,0:T(8,128)(2,1)S(1)}, bf16[768,256]{1,0:T(8,128)(2,1)S(1)}, f32[768,128]{1,0:T(8,128)S(1...) custom-call(s32[1]{0:T(128)} %bitcast.tp.side, ...), custom_call_target="tpu_custom_call" | custom-call | flops 1610612736 | bytes 1048576 | tf_op jit(solution)/shard_map/pallas_call | solution.py:254
  9.7 1.1 %collective-permute-start.3 = (bf16[208,128]{1,0:T(8,128)(2,1)S(1)}, bf16[208,128]{1,0:T(8,128)(2,1)S(1)}, u32[]{:S(2)}, u32[]{:S(2)}) collective-permute-start(bf16[208,128]{1,0:T(8,128)(2,1)S(1)} %get-tuple-element.62.refs_0_), channel_id=1, source_target_pairs={{0,24},{8,0},{16,8},{24,16},{1,25},{9,1},{17,9},{25,17},{2,26},{10... | collective-permute-start | bytes 159752 | tf_op jit(solution)/shard_map/ppermute | solution.py:645
  10.8 0.3 collective-permute-start.2
  11.2 0.7 %collective-permute-start.1 = (bf16[208,128]{1,0:T(8,128)(2,1)S(1)}, bf16[208,128]{1,0:T(8,128)(2,1)S(1)}, u32[]{:S(2)}, u32[]{:S(2)}) collective-permute-start(bf16[208,128]{1,0:T(8,128)(2,1)S(1)} %get-tuple-element.62.refs_0_), channel_id=1, source_target_pairs={{0,8},{8,16},{16,24},{24,0},{1,9},{9,17},{17,25},{25,1},{2,10},{10... | collective-permute-start | bytes 159752 | tf_op jit(solution)/shard_map/ppermute | solution.py:645
  11.9 2.7 %shard_map.129 = (bf16[768,384]{1,0:T(8,128)(2,1)S(1)}, bf16[768,384]{1,0:T(8,128)(2,1)S(1)}) custom-call(s32[1]{0:T(128)} %bitcast.tp.side, bf16[768,1024]{1,0:T(8,128)(2,1)S(1)} %get-tuple-element.58.own, bf16[768,1024]{1,0:T(8,128)(2,1)S(1)} %get-tuple-element.59.peer, f32[768,128]{1,0:T(8,128)S(1)} %get-tuple-element.60.inv, ...), custom_call_target="tpu_custom_call" | custom-call | flops 2415919104 | bytes 1048576 | tf_op jit(solution)/shard_map/pallas_call | solution.py:290
  14.6 0.8 %collective-permute-done.2.refs_2_ = bf16[208,128]{1,0:T(8,128)(2,1)S(1)} collective-permute-done((bf16[208,128]{1,0:T(8,128)(2,1)S(1)}, bf16[208,128]{1,0:T(8,128)(2,1)S(1)}, u32[]{:S(2)}, u32[]{:S(2)}) %collective-permute-start.2) | collective-permute-done | bytes 53280 | tf_op jit(solution)/shard_map/ppermute | solution.py:645
  15.4 1.7 %collective-permute-done.1.refs_1_ = bf16[208,128]{1,0:T(8,128)(2,1)S(1)} collective-permute-done((bf16[208,128]{1,0:T(8,128)(2,1)S(1)}, bf16[208,128]{1,0:T(8,128)(2,1)S(1)}, u32[]{:S(2)}, u32[]{:S(2)}) %collective-permute-start.1) | collective-permute-done | bytes 53280 | tf_op jit(solution)/shard_map/ppermute | solution.py:645
  17.1 0.1 shard_map.130
  17.2 0.7 %collective-permute-start.10 = (bf16[384,2048]{1,0:T(8,128)(2,1)S(1)}, bf16[384,2048]{1,0:T(8,128)(2,1)S(1)}, u32[]{:S(2)}, u32[]{:S(2)}) collective-permute-start(bf16[384,2048]{1,0:T(8,128)(2,1)S(1)} %copy-done.1), channel_id=1, source_target_pairs={{0,1},{1,0},{2,3},{3,2},{4,5},{5,4},{6,7},{7,6},{8,9},{9,8},{10,11... | collective-permute-start | bytes 4718600 | tf_op jit(solution)/shard_map/ppermute | solution.py:645
  18.0 5.6 %collective-permute-start.5 = (bf16[208,128]{1,0:T(8,128)(2,1)S(1)}, bf16[208,128]{1,0:T(8,128)(2,1)S(1)}, u32[]{:S(2)}, u32[]{:S(2)}) collective-permute-start(bf16[208,128]{1,0:T(8,128)(2,1)S(1)} %get-tuple-element.74.own), channel_id=1, source_target_pairs={{0,224},{32,0},{64,32},{96,64},{128,96},{160,128},{192,160},{224,1... | collective-permute-start | bytes 159752 | tf_op jit(solution)/shard_map/ppermute | solution.py:645
  23.6 2.1 %collective-permute-done.6.halo_ref = bf16[128,256]{1,0:T(8,128)(2,1)S(1)} collective-permute-done((bf16[128,256]{1,0:T(8,128)(2,1)S(1)}, bf16[128,256]{1,0:T(8,128)(2,1)S(1)}, u32[]{:S(2)}, u32[]{:S(2)}) %collective-permute-start.6) | collective-permute-done | bytes 65568 | tf_op jit(solution)/shard_map/ppermute | solution.py:684
  25.7 2.0 %shard_map.131 = bf16[384,384]{1,0:T(8,128)(2,1)S(1)} custom-call(s32[1]{0:T(128)} %bitcast.tp.side, s32[1]{0:T(128)} %bitcast.1.spot, bf16[768,384]{1,0:T(8,128)(2,1)S(1)} %get-tuple-element.71.q_ref, bf16[768,256]{1,0:T(8,128)(2,1)S(1)} %get-tuple-element.72.kv_ref, bf16[128,256]{1,0:T(8,128)(2,1)S(1)} %collective-permute-done.6.halo_ref, f32[6]{0:T(128)S(1)} %copy-done.6), custom_call_target="tpu_custom_call" | custom-call | flops 1073741824 | bytes 1048576 | tf_op jit(solution)/shard_map/pallas_call | solution.py:549
  27.7 1.1 %collective-permute-start.9 = (bf16[384,384]{1,0:T(8,128)(2,1)S(1)}, bf16[384,384]{1,0:T(8,128)(2,1)S(1)}, u32[]{:S(2)}, u32[]{:S(2)}) collective-permute-start(bf16[384,384]{1,0:T(8,128)(2,1)S(1)} %shard_map.131), channel_id=1, source_target_pairs={{0,1},{1,0},{2,3},{3,2},{4,5},{5,4},{6,7},{7,6},{8,9},{9,8},{10,11... | collective-permute-start | bytes 884744 | tf_op jit(solution)/shard_map/ppermute | solution.py:645
  28.9 4.4 %collective-permute-start.8 = (bf16[208,128]{1,0:T(8,128)(2,1)S(1)}, bf16[208,128]{1,0:T(8,128)(2,1)S(1)}, u32[]{:S(2)}, u32[]{:S(2)}) collective-permute-start(bf16[208,128]{1,0:T(8,128)(2,1)S(1)} %get-tuple-element.77), channel_id=1, source_target_pairs={{0,192},{32,224},{64,0},{96,32},{128,64},{160,96},{192,128},{224,1... | collective-permute-start | bytes 159752 | tf_op jit(solution)/shard_map/ppermute | solution.py:645
  33.2 2.0 %shard_map.133.a = bf16[384,384]{1,0:T(8,128)(2,1)S(1)} custom-call(s32[1]{0:T(128)} %bitcast.tp.side, s32[1]{0:T(128)} %bitcast.1.spot, bf16[768,384]{1,0:T(8,128)(2,1)S(1)} %get-tuple-element.71.q_ref, bf16[768,256]{1,0:T(8,128)(2,1)S(1)} %get-tuple-element.72.kv_ref, bf16[128,256]{1,0:T(8,128)(2,1)S(1)} %collective-permute-done.6.halo_ref, f32[6]{0:T(128)S(1)} %copy-done.6), custom_call_target="tpu_custom_call" | custom-call | flops 1073741824 | bytes 1048576 | tf_op jit(solution)/shard_map/pallas_call | solution.py:549
  35.3 2.0 %shard_map.135.in_ref = f32[768,384]{1,0:T(8,128)S(1)} custom-call(bf16[768,384]{1,0:T(8,128)(2,1)S(1)} %get-tuple-element.82.q_ref, bf16[768,384]{1,0:T(8,128)(2,1)S(1)} %get-tuple-element.84.k_ref, bf16[768,384]{1,0:T(8,128)(2,1)S(1)} %get-tuple-element.85.v_ref, f32[8,768]{1,0:T(8,128)S(1)} %get-tuple-element.86.row_ref, ...), custom_call_target="tpu_custom_call" | custom-call | flops 3221225472 | bytes 1048576 | tf_op jit(solution)/shard_map/pallas_call | solution.py:343
  37.3 1.4 %shard_map.134.refs_7_ = f32[384,2048]{1,0:T(8,128)S(1)} custom-call(bf16[384,384]{1,0:T(8,128)(2,1)S(1)} %shard_map.133.a, bf16[384,384]{1,0:T(8,128)(2,1)S(1)} %collective-permute-done.9.b, bf16[384,2048]{1,0:T(8,128)(2,1)S(1)} %copy-done.1, bf16[384,2048]{1,0:T(8,128)(2,1)S(1)} %collective-permute-done.10.wb), custom_call_target="tpu_custom_call" | custom-call | flops 1207959552 | bytes 1048576 | tf_op jit(solution)/shard_map/pallas_call | solution.py:594
  38.8 1.4 %collective-permute-done.7.refs_4_ = bf16[208,128]{1,0:T(8,128)(2,1)S(1)} collective-permute-done((bf16[208,128]{1,0:T(8,128)(2,1)S(1)}, bf16[208,128]{1,0:T(8,128)(2,1)S(1)}, u32[]{:S(2)}, u32[]{:S(2)}) %collective-permute-start.7) | collective-permute-done | bytes 53280 | tf_op jit(solution)/shard_map/ppermute | solution.py:645
  40.2 0.7 %shard_map.136 = bf16[384,384]{1,0:T(8,128)(2,1)S(1)} custom-call(s32[1]{0:T(128)} %bitcast.tp.side, s32[1]{0:T(128)} %bitcast.2.place.row, bf16[768,384]{1,0:T(8,128)(2,1)S(1)} %get-tuple-element.82.q_ref, f32[768,384]{1,0:T(8,128)S(1)} %shard_map.135.in_ref, f32[768,384]{1,0:T(8,128)S(1)} %get-tuple-element.55.col.col_ref, f32[384]{0:T(512)S(1)} %copy-done.2, ...), custom_call_target="tpu_custom_call" | custom-call | flops 536870912 | bytes 1048576 | tf_op jit(solution)/shard_map/pallas_call | solution.py:475
  40.9 0.8 %collective-permute-start.11 = (bf16[384,384]{1,0:T(8,128)(2,1)S(1)}, bf16[384,384]{1,0:T(8,128)(2,1)S(1)}, u32[]{:S(2)}, u32[]{:S(2)}) collective-permute-start(bf16[384,384]{1,0:T(8,128)(2,1)S(1)} %shard_map.136), channel_id=1, source_target_pairs={{0,1},{1,0},{2,3},{3,2},{4,5},{5,4},{6,7},{7,6},{8,9},{9,8},{10,11... | collective-permute-start | bytes 884744 | tf_op jit(solution)/shard_map/ppermute | solution.py:645
  41.7 1.5 %shard_map.137.more = f32[384,2048]{1,0:T(8,128)S(1)} custom-call(s32[1]{0:T(128)} %bitcast.tp.side, s32[1]{0:T(128)} %bitcast.2.place.row, bf16[768,384]{1,0:T(8,128)(2,1)S(1)} %get-tuple-element.82.q_ref, f32[768,384]{1,0:T(8,128)S(1)} %shard_map.135.in_ref, f32[768,384]{1,0:T(8,128)S(1)} %get-tuple-element.55.col.col_ref, f32[384]{0:T(512)S(1)} %copy-done.2, ...), custom_call_target="tpu_custom_call" | custom-call | flops 536870912 | bytes 1048576 | tf_op jit(solution)/shard_map/pallas_call | solution.py:616
  43.3 1.9 %shard_map.138 = bf16[384,2048]{1,0:T(8,128)(2,1)} custom-call(bf16[384,384]{1,0:T(8,128)(2,1)S(1)} %collective-permute-done.11.a, bf16[384,2048]{1,0:T(8,128)(2,1)S(1)} %collective-permute-done.12.w, f32[384,2048]{1,0:T(8,128)S(1)} %shard_map.137.more), custom_call_target="tpu_custom_call" | custom-call | flops 603979776 | bytes 1048576 | tf_op jit(solution)/shard_map/pallas_call | solution.py:631
  (28 shorter events, 0.2 us)
Async XLA Ops:
  0.0 7.2 %collective-permute-start = (bf16[768,1024]{1,0:T(8,128)(2,1)}, bf16[768,1024]{1,0:T(8,128)(2,1)S(1)}, u32[]{:S(2)}, u32[]{:S(2)}) collective-permute-start(bf16[768,1024]{1,0:T(8,128)(2,1)} %bitcast.10), channel_id=1, source_target_pairs={{0,1},{1,0},{2,3},{3,2},{4,5},{5,4},{6,7},{7,6},{8,9},{9,8},{10,11... | collective-permute-start | bytes 4718600 | tf_op jit(solution)/shard_map/ppermute | solution.py:645
  3.2 4.0 %copy-start.3 = (f32[2048]{0:T(1024)S(1)}, f32[2048]{0:T(1024)}, u32[]{:S(2)}) copy-start(f32[2048]{0:T(1024)} %param.14) | copy-start | bytes 24580
  7.2 4.7 %copy-start.4 = (bf16[2048,384]{1,0:T(8,128)(2,1)S(1)}, bf16[2048,384]{1,0:T(8,128)(2,1)}, u32[]{:S(2)}) copy-start(bf16[2048,384]{1,0:T(8,128)(2,1)} %w0.1) | copy-start | bytes 4718596
  7.2 4.7 %copy-start.5 = (bf16[2048,384]{1,0:T(8,128)(2,1)S(1)}, bf16[2048,384]{1,0:T(8,128)(2,1)}, u32[]{:S(2)}) copy-start(bf16[2048,384]{1,0:T(8,128)(2,1)} %w1.1) | copy-start | bytes 4718596
  9.7 4.8 %collective-permute-start.3 = (bf16[208,128]{1,0:T(8,128)(2,1)S(1)}, bf16[208,128]{1,0:T(8,128)(2,1)S(1)}, u32[]{:S(2)}, u32[]{:S(2)}) collective-permute-start(bf16[208,128]{1,0:T(8,128)(2,1)S(1)} %get-tuple-element.62.refs_0_), channel_id=1, source_target_pairs={{0,24},{8,0},{16,8},{24,16},{1,25},{9,1},{17,9},{25,17},{2,26},{10... | collective-permute-start | bytes 159752 | tf_op jit(solution)/shard_map/ppermute | solution.py:645
  10.8 4.5 %collective-permute-start.2 = (bf16[208,128]{1,0:T(8,128)(2,1)S(1)}, bf16[208,128]{1,0:T(8,128)(2,1)S(1)}, u32[]{:S(2)}, u32[]{:S(2)}) collective-permute-start(bf16[208,128]{1,0:T(8,128)(2,1)S(1)} %get-tuple-element.62.refs_0_), channel_id=1, source_target_pairs={{0,16},{8,24},{16,0},{24,8},{1,17},{9,25},{17,1},{25,9},{2,18},{10... | collective-permute-start | bytes 159752 | tf_op jit(solution)/shard_map/ppermute | solution.py:645
  11.2 5.9 %collective-permute-start.1 = (bf16[208,128]{1,0:T(8,128)(2,1)S(1)}, bf16[208,128]{1,0:T(8,128)(2,1)S(1)}, u32[]{:S(2)}, u32[]{:S(2)}) collective-permute-start(bf16[208,128]{1,0:T(8,128)(2,1)S(1)} %get-tuple-element.62.refs_0_), channel_id=1, source_target_pairs={{0,8},{8,16},{16,24},{24,0},{1,9},{9,17},{17,25},{25,1},{2,10},{10... | collective-permute-start | bytes 159752 | tf_op jit(solution)/shard_map/ppermute | solution.py:645
  11.9 5.4 %copy-start.1 = (bf16[384,2048]{1,0:T(8,128)(2,1)S(1)}, bf16[384,2048]{1,0:T(8,128)(2,1)}, u32[]{:S(2)}) copy-start(bf16[384,2048]{1,0:T(8,128)(2,1)} %wa.1) | copy-start | bytes 4718596
  11.9 6.1 %copy-start = (bf16[384,2048]{1,0:T(8,128)(2,1)S(1)}, bf16[384,2048]{1,0:T(8,128)(2,1)}, u32[]{:S(2)}) copy-start(bf16[384,2048]{1,0:T(8,128)(2,1)} %refs_6_.1) | copy-start | bytes 4718596
  11.9 13.8 %copy-start.6 = (f32[6]{0:T(128)S(1)}, f32[6]{0:T(128)}, u32[]{:S(2)}) copy-start(f32[6]{0:T(128)} %sink_ref.3) | copy-start | bytes 76
  17.2 20.1 %collective-permute-start.10 = (bf16[384,2048]{1,0:T(8,128)(2,1)S(1)}, bf16[384,2048]{1,0:T(8,128)(2,1)S(1)}, u32[]{:S(2)}, u32[]{:S(2)}) collective-permute-start(bf16[384,2048]{1,0:T(8,128)(2,1)S(1)} %copy-done.1), channel_id=1, source_target_pairs={{0,1},{1,0},{2,3},{3,2},{4,5},{5,4},{6,7},{7,6},{8,9},{9,8},{10,11... | collective-permute-start | bytes 4718600 | tf_op jit(solution)/shard_map/ppermute | solution.py:645
  17.9 25.3 %collective-permute-start.12 = (bf16[384,2048]{1,0:T(8,128)(2,1)S(1)}, bf16[384,2048]{1,0:T(8,128)(2,1)S(1)}, u32[]{:S(2)}, u32[]{:S(2)}) collective-permute-start(bf16[384,2048]{1,0:T(8,128)(2,1)S(1)} %copy-done), channel_id=1, source_target_pairs={{0,1},{1,0},{2,3},{3,2},{4,5},{5,4},{6,7},{7,6},{8,9},{9,8},{10,11... | collective-permute-start | bytes 4718600 | tf_op jit(solution)/shard_map/ppermute | solution.py:645
  18.0 7.6 %collective-permute-start.6 = (bf16[128,256]{1,0:T(8,128)(2,1)S(1)}, bf16[128,256]{1,0:T(8,128)(2,1)S(1)}, u32[]{:S(2)}, u32[]{:S(2)}) collective-permute-start(bf16[128,256]{1,0:T(8,128)(2,1)S(1)} %get-tuple-element.73), channel_id=1, source_target_pairs={{0,8},{8,16},{16,24},{24,32},{32,40},{40,48},{48,56},{56,64},{64,7... | collective-permute-start | bytes 196616 | tf_op jit(solution)/shard_map/ppermute | solution.py:684
  18.0 10.7 %collective-permute-start.5 = (bf16[208,128]{1,0:T(8,128)(2,1)S(1)}, bf16[208,128]{1,0:T(8,128)(2,1)S(1)}, u32[]{:S(2)}, u32[]{:S(2)}) collective-permute-start(bf16[208,128]{1,0:T(8,128)(2,1)S(1)} %get-tuple-element.74.own), channel_id=1, source_target_pairs={{0,224},{32,0},{64,32},{96,64},{128,96},{160,128},{192,160},{224,1... | collective-permute-start | bytes 159752 | tf_op jit(solution)/shard_map/ppermute | solution.py:645
  23.6 5.2 %collective-permute-start.4 = (bf16[208,128]{1,0:T(8,128)(2,1)S(1)}, bf16[208,128]{1,0:T(8,128)(2,1)S(1)}, u32[]{:S(2)}, u32[]{:S(2)}) collective-permute-start(bf16[208,128]{1,0:T(8,128)(2,1)S(1)} %get-tuple-element.74.own), channel_id=1, source_target_pairs={{0,32},{32,64},{64,96},{96,128},{128,160},{160,192},{192,224},{224... | collective-permute-start | bytes 159752 | tf_op jit(solution)/shard_map/ppermute | solution.py:645
  27.7 9.6 %collective-permute-start.9 = (bf16[384,384]{1,0:T(8,128)(2,1)S(1)}, bf16[384,384]{1,0:T(8,128)(2,1)S(1)}, u32[]{:S(2)}, u32[]{:S(2)}) collective-permute-start(bf16[384,384]{1,0:T(8,128)(2,1)S(1)} %shard_map.131), channel_id=1, source_target_pairs={{0,1},{1,0},{2,3},{3,2},{4,5},{5,4},{6,7},{7,6},{8,9},{9,8},{10,11... | collective-permute-start | bytes 884744 | tf_op jit(solution)/shard_map/ppermute | solution.py:645
  28.9 9.9 %collective-permute-start.8 = (bf16[208,128]{1,0:T(8,128)(2,1)S(1)}, bf16[208,128]{1,0:T(8,128)(2,1)S(1)}, u32[]{:S(2)}, u32[]{:S(2)}) collective-permute-start(bf16[208,128]{1,0:T(8,128)(2,1)S(1)} %get-tuple-element.77), channel_id=1, source_target_pairs={{0,192},{32,224},{64,0},{96,32},{128,64},{160,96},{192,128},{224,1... | collective-permute-start | bytes 159752 | tf_op jit(solution)/shard_map/ppermute | solution.py:645
  33.2 7.0 %collective-permute-start.7 = (bf16[208,128]{1,0:T(8,128)(2,1)S(1)}, bf16[208,128]{1,0:T(8,128)(2,1)S(1)}, u32[]{:S(2)}, u32[]{:S(2)}) collective-permute-start(bf16[208,128]{1,0:T(8,128)(2,1)S(1)} %get-tuple-element.77), channel_id=1, source_target_pairs={{0,96},{32,128},{64,160},{96,192},{128,224},{160,0},{192,32},{224,... | collective-permute-start | bytes 159752 | tf_op jit(solution)/shard_map/ppermute | solution.py:645
  37.3 2.9 %copy-start.2 = (f32[384]{0:T(512)S(1)}, f32[384]{0:T(512)}, u32[]{:S(2)}) copy-start(f32[384]{0:T(512)} %gain.3) | copy-start | bytes 4612
  40.9 2.4 %collective-permute-start.11 = (bf16[384,384]{1,0:T(8,128)(2,1)S(1)}, bf16[384,384]{1,0:T(8,128)(2,1)S(1)}, u32[]{:S(2)}, u32[]{:S(2)}) collective-permute-start(bf16[384,384]{1,0:T(8,128)(2,1)S(1)} %shard_map.136), channel_id=1, source_target_pairs={{0,1},{1,0},{2,3},{3,2},{4,5},{5,4},{6,7},{7,6},{8,9},{9,8},{10,11... | collective-permute-start | bytes 884744 | tf_op jit(solution)/shard_map/ppermute | solution.py:645
